TPU v7x, 256 devices: a 4x2x16 block of a 4x16x16 slice. The times are simulated.
256 devices in a mesh: grp: 2 (over y), fs: 32 (over z, core), tp: 4 (over x).
Axes of the slice: x: 4, y: 2, z: 16, core: 2. Of those that a mesh axis runs over, the one named last changes fastest.
The devices are a block of a 4x16x16 slice.
Arguments:
- tokens: bfloat16 [14336, 2048], P(('grp', 'fs'), 'tp'), parts along dimension 0, may hold values from -170 to 170
- routes: int32 [14336, 6], P(('grp', 'fs')), parts along dimension 0, may hold values from 0 to 63, all different within a row; in each aligned block of 224 rows (0 to 223, 224 to 447, ...) at most 28 rows name the same one
- route_weights: float32 [14336, 6], P(('grp', 'fs')), parts along dimension 0, may hold values from 0.2 to 1
- norm_gain: float32 [2048], P('fs'), may hold values from 0.1 to 1.9
- gate_experts: float32 [64, 2048, 512], P(None, 'fs', 'tp'), may hold values from -0.125 to 0.125
- up_experts: float32 [64, 2048, 512], P(None, 'fs', 'tp'), may hold values from -0.125 to 0.125
- down_experts: float32 [64, 512, 2048], P(None, 'fs', 'tp'), may hold values from -0.25 to 0.25
- shared_gate: float32 [2048, 512], P('fs', 'tp'), may hold values from -0.125 to 0.125
- shared_up: float32 [2048, 512], P('fs', 'tp'), may hold values from -0.125 to 0.125
- shared_down: float32 [512, 2048], P('fs', 'tp'), may hold values from -0.25 to 0.25
Outputs:
- mixed: bfloat16 [14336, 2048], P(('grp', 'fs'), 'tp'), parts along dimension 0
- gate_ready: bfloat16 [128, 2048, 512], P(('grp', 'fs'), None, 'tp'), parts along dimension 0
- up_ready: bfloat16 [128, 2048, 512], P(('grp', 'fs'), None, 'tp'), parts along dimension 0
- down_ready: bfloat16 [128, 512, 2048], P(('grp', 'fs'), 'tp'), parts along dimension 0
- shared_gate_ready: bfloat16 [4096, 512], P('grp', 'tp'), parts along dimension 0
- shared_up_ready: bfloat16 [4096, 512], P('grp', 'tp'), parts along dimension 0
- shared_down_ready: bfloat16 [1024, 2048], P(('grp', 'tp')), parts along dimension 0
There are 2 independent parts, one for each index of `grp`. A program takes and returns all parts, laid end to end along the dimension named above; an argument that names none is the same for every part. Nothing has to cross between parts.
Inputs may be any that keep to these rules, and one draw needn't show every extreme that they name: `routes`: the 6 experts of a row differ; among the rows of one index of fs no expert is named more than 28 times, a bound that some block reaches.
All inputs are finite; a program needn't handle non-finite values.
Results may differ from a plain program's by a relative error of at most 0.013.
Values may be sent and summed in bfloat16 or wider, within the bound.
A program may use at most 128 MiB of HBM per device.

v0:
```python
import jax
import jax.numpy as jnp
from jax import lax
from jax.sharding import PartitionSpec as P


def in_one_piece(arrays, axis, split_dim, concat_dim, along):
    widths = [a.shape[along] for a in arrays]
    both = jnp.concatenate(arrays, axis=along)
    out = lax.all_to_all(both, axis, split_axis=split_dim, concat_axis=concat_dim, tiled=True)
    return tuple(jnp.split(out, [sum(widths[:k]) for k in range(1, len(widths))], axis=along))


def in_one_piece_2(arrays, axis, dim, along):
    ends, at = ([], 0)
    for a in arrays[:-1]:
        at += a.shape[along]
        ends.append(at)
    both = jnp.concatenate(arrays, axis=along)
    return tuple(jnp.split(lax.all_gather(both, axis, axis=dim, tiled=True), ends, axis=along))


def sent_to_all(x, axis):
    size = lax.axis_size(axis)
    return lax.all_to_all(jnp.broadcast_to(x[None], (size, *x.shape)), axis, 0, 0, tiled=True)


def in_order(blocks, dim):
    blocks = jnp.moveaxis(blocks, 0, dim)
    dims = blocks.shape
    return blocks.reshape(*dims[:dim], dims[dim] * dims[dim + 1], *dims[dim + 2 :])


def collect(x, axis, dim):
    blocks = sent_to_all(x, axis)
    return in_order(blocks, dim)


def split_up(x, dim, size):
    dims = x.shape
    blocks = x.reshape(*dims[:dim], size, dims[dim] // size, *dims[dim + 1 :])
    return jnp.moveaxis(blocks, dim, 0)


def summed_on_arrival(x, axis, dim):
    size = lax.axis_size(axis)
    blocks = lax.all_to_all(split_up(x, dim, size), axis, 0, 0, tiled=True)
    return jnp.sum(blocks.astype(jnp.float32), axis=0)


def per_device(
    tokens,
    routes,
    route_weights,
    norm_gain,
    gate_experts,
    up_experts,
    down_experts,
    shared_gate,
    shared_up,
    shared_down,
):
    gain_rows = norm_gain[None, :, None]
    gate_cast = (gate_experts * gain_rows).astype(jnp.bfloat16)
    up_cast = (up_experts * gain_rows).astype(jnp.bfloat16)
    down_cast = down_experts.astype(jnp.bfloat16)
    gate_local, up_local = in_one_piece((gate_cast, up_cast), "fs", 0, 1, 2)
    down_local = lax.all_to_all(
        lax.all_to_all(down_cast, "fs", split_axis=0, concat_axis=1, tiled=True),
        "tp",
        split_axis=1,
        concat_axis=2,
        tiled=True,
    )
    shared_gate_cast = (shared_gate * norm_gain[:, None]).astype(jnp.bfloat16)
    shared_up_cast = (shared_up * norm_gain[:, None]).astype(jnp.bfloat16)
    shared_down_cast = shared_down.astype(jnp.bfloat16)
    shared_gate_local, shared_up_local, shared_down_rows = (
        *in_one_piece_2((shared_gate_cast, shared_up_cast), "fs", 0, 1),
        lax.all_gather(shared_down_cast, "fs", axis=0, tiled=True),
    )
    shared_down_local = lax.all_to_all(
        shared_down_rows, "tp", split_axis=0, concat_axis=1, tiled=True
    )
    gathered = collect(tokens, "tp", 1)
    widened = gathered.astype(jnp.float32)
    normed = (
        widened * lax.rsqrt(jnp.mean(widened * widened, axis=1, keepdims=True) + 1e-06)
    ).astype(jnp.bfloat16)
    shared_active = (
        jax.nn.silu(jnp.dot(normed, shared_gate_local, preferred_element_type=jnp.float32))
        * jnp.dot(normed, shared_up_local, preferred_element_type=jnp.float32)
    ).astype(jnp.bfloat16)
    shared_rows = summed_on_arrival(
        jnp.dot(shared_active, shared_down_local, preferred_element_type=jnp.float32).astype(
            jnp.bfloat16
        ),
        "tp",
        1,
    )
    tok_rows, top_count = routes.shape
    experts_all = gate_experts.shape[0]
    capacity = 4 * tok_rows * top_count // (3 * experts_all)
    fs_count = lax.axis_size("fs")
    held = experts_all // fs_count
    quarter = tokens.shape[1]
    flat_routes = routes.reshape(-1)
    onehot = (flat_routes[:, None] == jnp.arange(experts_all, dtype=jnp.int32)[None, :]).astype(
        jnp.int32
    )
    earlier = jnp.cumsum(onehot, axis=0) - onehot
    slot_index = jnp.sum(earlier * onehot, axis=1)
    target = flat_routes * capacity + slot_index
    source = (
        jnp.full((experts_all * capacity,), -1, jnp.int32)
        .at[target]
        .set(jnp.arange(tok_rows * top_count, dtype=jnp.int32) // top_count)
    )
    present = (source >= 0)[:, None]
    safe_source = jnp.maximum(source, 0)
    own_part = lax.dynamic_slice_in_dim(normed, lax.axis_index("tp") * quarter, quarter, 1)
    send_rows = jnp.where(present, own_part[safe_source], jnp.zeros((), jnp.bfloat16))
    send_rows = send_rows.reshape(fs_count, held, capacity, quarter)
    received = lax.all_to_all(send_rows, "fs", split_axis=0, concat_axis=0, tiled=True)
    received = lax.all_gather(received, "tp", axis=3, tiled=True)
    gate_hidden = jnp.einsum(
        "sjcd,jdf->sjcf", received, gate_local, preferred_element_type=jnp.float32
    )
    up_hidden = jnp.einsum("sjcd,jdf->sjcf", received, up_local, preferred_element_type=jnp.float32)
    active = (jax.nn.silu(gate_hidden) * up_hidden).astype(jnp.bfloat16)
    partial_rows = jnp.einsum(
        "sjcf,jfd->sjcd", active, down_local, preferred_element_type=jnp.float32
    )
    summed = lax.psum_scatter(
        partial_rows.astype(jnp.bfloat16), "tp", scatter_dimension=3, tiled=True
    )
    returned = lax.all_to_all(summed, "fs", split_axis=0, concat_axis=0, tiled=True)
    picked = returned.reshape(experts_all * capacity, quarter)[target].reshape(
        tok_rows, top_count, quarter
    )
    weighted = jnp.einsum("tkd,tk->td", picked.astype(jnp.float32), route_weights)
    mixed = (weighted + shared_rows).astype(jnp.bfloat16)
    return (
        mixed,
        gate_local,
        up_local,
        down_local,
        shared_gate_local,
        shared_up_local,
        shared_down_local,
    )


def solution(mesh):
    return jax.shard_map(
        per_device,
        mesh=mesh,
        in_specs=(
            P(("grp", "fs"), "tp"),
            P(("grp", "fs"), None),
            P(("grp", "fs"), None),
            P("fs"),
            P(None, "fs", "tp"),
            P(None, "fs", "tp"),
            P(None, "fs", "tp"),
            P("fs", "tp"),
            P("fs", "tp"),
            P("fs", "tp"),
        ),
        out_specs=(
            P(("grp", "fs"), "tp"),
            P(("grp", "fs"), None, "tp"),
            P(("grp", "fs"), None, "tp"),
            P(("grp", "fs"), "tp", None),
            P("grp", "tp"),
            P("grp", "tp"),
            P(("grp", "tp"), None),
        ),
        check_vma=False,
    )
```

profile of v0, /device:TPU:38, one launch (start us, length us, event | category | flops | bytes accessed | tf_op | source)
XLA Modules:
  0.0 608.0 jit_solution(14594618923926960807)
XLA Ops:
  7.2 1.9 broadcast_in_dim.37
  9.1 22.6 %all-to-all-start.1 = ((bf16[4,224,512]{2,1,0:T(8,128)(2,1)}), bf16[4,224,512]{2,1,0:T(8,128)(2,1)S(1)}, u32[]{:S(2)}, u32[]{:S(2)}) async-start(bf16[4,224,512]{2,1,0:T(8,128)(2,1)} %broadcast_in_dim.37), calls=%async_computation.1 | async-start | bytes 1835008 | tf_op jit(solution)/shard_map/all_to_all | solution.py:25
  31.9 0.1 eq.22
  32.2 18.1 %reduce-window.6 = s32[64,11,128]{2,1,0:T(8,128)S(1)} reduce-window(s32[64,11,128]{2,1,0:T(8,128)S(1)} %reshape.94, s32[]{:T(128)} %constant.18.clone.1), window={size=1x1x128 pad=0_0x0_0x127_0}, to_apply=%region_0.0 | reduce-window | flops 11444224 | bytes 720900 | tf_op jit(solution)/shard_map/reduce-window
  50.3 0.2 slice.16
  50.5 0.3 copy.71
  50.9 0.2 broadcast_add_fusion
  51.3 0.1 copy.69
  51.5 0.1 mul.82
  51.7 7.6 %scatter_custom_fusion = s32[1792]{0:T(1024)S(1)} fusion(s32[1344]{0:T(1024)S(1)} %fusion.26, s32[1344]{0:T(1024)S(1)} %add_select_fusion, s32[]{:T(128)} %constant.15.clone.1), kind=kCustom, calls=%fused_computation.63 | custom fusion | bytes 7172 | tf_op jit(solution)/shard_map/scatter | solution.py:117
  59.5 0.2 convert_bitcast_fusion.1
  59.7 0.2 copy.91
  59.9 0.3 fusion
  60.2 0.2 multiply_convert_fusion.2
  60.4 6.1 %gather_fusion = bf16[1792,512]{1,0:T(8,128)(2,1)} fusion(bf16[224,512]{1,0:T(8,128)(2,1)S(1)} %constant_dynamic-slice_fusion, s32[2048]{0:T(1024)S(1)} %pad_clamp_fusion.1), kind=kCustom, calls=%fused_computation | custom fusion | bytes 3677184 | tf_op jit(solution)/shard_map/gather | solution.py:122
  66.5 2.4 gather.9
  68.9 0.4 broadcast_select_fusion
  69.4 3.2 copy.74
  72.5 6.8 %all-to-all-start.2 = ((bf16[32,2,28,512]{3,1,2,0:T(2,128)(2,1)}), bf16[32,2,28,512]{3,1,2,0:T(2,128)(2,1)S(1)}, u32[]{:S(2)}, u32[]{:S(2)}) async-start(bf16[32,2,28,512]{3,1,2,0:T(2,128)(2,1)} %copy.74), calls=%async_computation.2 | async-start | bytes 3670016 | tf_op jit(solution)/shard_map/all_to_all | solution.py:124
  79.3 2.7 convert_element_type.69
  82.1 85.9 %all-to-all-done.2 = bf16[32,2,28,512]{3,1,2,0:T(2,128)(2,1)S(1)} async-done(((bf16[32,2,28,512]{3,1,2,0:T(2,128)(2,1)}), bf16[32,2,28,512]{3,1,2,0:T(2,128)(2,1)S(1)}, u32[]{:S(2)}, u32[]{:S(2)}) %all-to-all-start.2) | async-done | bytes 1835040 | tf_op jit(solution)/shard_map/all_to_all | solution.py:124
  168.0 5.5 all-to-all-start.3
  173.5 1.9 copy.75
  175.5 53.7 %all-to-all-done.3 = bf16[64,16,512]{2,1,0:T(8,128)(2,1)} async-done(((bf16[64,16,512]{2,1,0:T(8,128)(2,1)}), bf16[64,16,512]{2,1,0:T(8,128)(2,1)}, u32[]{:S(2)}, u32[]{:S(2)}) %all-to-all-start.3) | async-done | bytes 1048608 | tf_op jit(solution)/shard_map/all_to_all | solution.py:69
  229.2 1.3 copy.76
  230.6 2.0 copy.77
  232.6 4.8 all-to-all-start.4
  237.4 2.9 multiply_convert_fusion.1
  240.4 1.6 pad_maximum_fusion
  242.0 20.5 %all-to-all-done.4 = bf16[2,512,512]{2,0,1:T(2,128)(2,1)S(1)} async-done(((bf16[2,512,512]{2,0,1:T(2,128)(2,1)}), bf16[2,512,512]{2,0,1:T(2,128)(2,1)S(1)}, u32[]{:S(2)}, u32[]{:S(2)}) %all-to-all-start.4) | async-done | bytes 1048608 | tf_op jit(solution)/shard_map/all_to_all | solution.py:68
  262.5 5.6 all-to-all-start
  268.3 0.6 pad_maximum_fusion.1
  269.0 0.2 copy.78
  269.2 1.8 copy.79
  271.0 1.8 reshape.123
  272.8 101.3 %all-to-all-done = bf16[64,64,256]{2,1,0:T(8,128)(2,1)} async-done(((bf16[64,64,256]{2,1,0:T(8,128)(2,1)}), bf16[64,64,256]{2,1,0:T(8,128)(2,1)}, u32[]{:S(2)}, u32[]{:S(2)}) %all-to-all-start) | async-done | bytes 2097184 | tf_op jit(solution)/shard_map/all_to_all | solution.py:10
  374.1 1.7 copy.68
  375.9 1.7 fusion.31
  377.5 6.4 %convolution_bitcast_fusion.1 = f32[32,2,28,128]{3,0,2,1:T(8,128)} fusion(bf16[32,2,28,2048]{3,0,2,1:T(8,128)(2,1)} %all-gather.3.cloned.1.call-done, bf16[2,2048,128]{2,1,0:T(8,128)(2,1)} %get-tuple-element.21), kind=kOutput, calls=%fused_computation.15 | convolution fusion | flops 939524096 | bytes 9306112 | tf_op jit(solution)/shard_map/sjcd,jdf->sjcf/dot_general | solution.py:126
  384.0 11.9 %convert_bitcast_fusion = bf16[32,2,28,2048]{3,0,2,1:T(8,128)(2,1)} fusion(bf16[32,2,28,2048]{3,0,2,1:T(8,128)(2,1)} %all-gather.3.cloned.1.call-done, bf16[2,2048,128]{2,1,0:T(8,128)(2,1)} %get-tuple-element.22, bf16[2,128,2048,1]{2,1,0,3:T(8,128)(2,1)S(1)} %reshape.123, f32[32,2,28,128]{3,0,2,1:T(8,128)} %convolution_bitcast_fusion.1), kind=kOutput, calls=%fused_computation.3 | convolution fusion | flops 1884094464 | bytes 17694720 | tf_op jit(solution)/shard_map/sjcf,jfd->sjcd/dot_general | solution.py:131
  395.9 0.7 copy-done.3
  396.6 28.3 %all_gather.11 = bf16[512,512]{1,0:T(8,128)(2,1)S(1)} all-gather(bf16[16,512]{1,0:T(8,128)(2,1)S(1)} %convert_element_type.75), channel_id=1, replica_groups=mesh['grp'=2,'fs'=32,'tp'=4] {'fs'}, dimensions={0}, use_global_device_ids=true | all-gather | bytes 540672 | tf_op jit(solution)/shard_map/all_gather | solution.py:80
  424.9 18.7 %all_to_all.93 = bf16[4,128,512]{2,1,0:T(8,128)(2,1)S(1)} all-to-all(bf16[4,128,512]{2,1,0:T(8,128)(2,1)S(1)} %bitcast.86), channel_id=1, replica_groups=mesh['grp'=2,'fs'=32,'tp'=4] {'tp'}, dimensions={0} | all-to-all | bytes 1048576 | tf_op jit(solution)/shard_map/all_to_all | solution.py:82
  443.6 0.3 copy.82
  443.9 2.1 fusion.32
  446.0 0.4 fusion.34
  446.4 0.4 copy-done
  446.8 1.7 convolution_convert_fusion
  448.5 1.0 copy.97
  449.5 5.6 all-to-all-start.7
  455.1 24.8 %reduce-scatter.2.cloned.1.call-done = bf16[32,2,28,512]{3,0,2,1:T(8,128)(2,1)} async-done(((bf16[32,2,28,2048]{3,0,2,1:T(8,128)(2,1)}), bf16[32,2,28,512]{3,0,2,1:T(8,128)(2,1)}) %reduce-scatter.2.cloned.1.call-update) | async-done | bytes 1835024 | tf_op jit(solution)/shard_map/reduce_scatter | solution.py:134
  479.9 4.6 copy.80
  484.6 13.3 %all-to-all-start.5 = ((bf16[32,2,28,512]{3,1,2,0:T(2,128)(2,1)}), bf16[32,2,28,512]{3,1,2,0:T(2,128)(2,1)}, u32[]{:S(2)}, u32[]{:S(2)}) async-start(bf16[32,2,28,512]{3,1,2,0:T(2,128)(2,1)} %copy.80), calls=%async_computation.6 | async-start | bytes 3670016 | tf_op jit(solution)/shard_map/all_to_all | solution.py:137
  497.9 0.2 copy.88
  498.1 1.0 copy.84
  499.1 0.1 convert_reduce_fusion
  499.2 1.1 copy.92
  500.3 86.3 %all-to-all-done.5 = bf16[32,2,28,512]{3,1,2,0:T(2,128)(2,1)} async-done(((bf16[32,2,28,512]{3,1,2,0:T(2,128)(2,1)}), bf16[32,2,28,512]{3,1,2,0:T(2,128)(2,1)}, u32[]{:S(2)}, u32[]{:S(2)}) %all-to-all-start.5) | async-done | bytes 1835040 | tf_op jit(solution)/shard_map/all_to_all | solution.py:137
  586.6 3.3 copy.81
  589.9 2.5 reshape.91
  592.4 5.3 gather_fusion.1
  597.7 2.4 reshape.92
  600.1 0.6 fusion.33
  600.7 0.8 fusion.13
  (42 shorter events, 1.3 us)
Async XLA Ops:
  7.2 24.5 %copy-start.4 = (s32[224,6]{0,1:T(8,128)S(1)}, s32[224,6]{0,1:T(8,128)}, u32[]{:S(2)}) copy-start(s32[224,6]{0,1:T(8,128)} %param.11) | copy-start | bytes 16132
  9.1 50.3 %all-to-all-start.1 = ((bf16[4,224,512]{2,1,0:T(8,128)(2,1)}), bf16[4,224,512]{2,1,0:T(8,128)(2,1)S(1)}, u32[]{:S(2)}, u32[]{:S(2)}) async-start(bf16[4,224,512]{2,1,0:T(8,128)(2,1)} %broadcast_in_dim.37), calls=%async_computation.1 | async-start | bytes 1835008 | tf_op jit(solution)/shard_map/all_to_all | solution.py:25
  72.5 95.5 %all-to-all-start.2 = ((bf16[32,2,28,512]{3,1,2,0:T(2,128)(2,1)}), bf16[32,2,28,512]{3,1,2,0:T(2,128)(2,1)S(1)}, u32[]{:S(2)}, u32[]{:S(2)}) async-start(bf16[32,2,28,512]{3,1,2,0:T(2,128)(2,1)} %copy.74), calls=%async_computation.2 | async-start | bytes 3670016 | tf_op jit(solution)/shard_map/all_to_all | solution.py:124
  168.0 61.3 %all-to-all-start.3 = ((bf16[64,16,512]{2,1,0:T(8,128)(2,1)}), bf16[64,16,512]{2,1,0:T(8,128)(2,1)}, u32[]{:S(2)}, u32[]{:S(2)}) async-start(bf16[64,16,512]{2,1,0:T(8,128)(2,1)} %convert_element_type.69), calls=%async_computation.3 | async-start | bytes 2097152 | tf_op jit(solution)/shard_map/all_to_all | solution.py:69
  173.4 204.1 %all-gather.3.cloned.1.call-start = ((), (), s32[]{:S(2)}) async-start(), calls=%async_computation.9 | async-start | bytes 9175040 | tf_op jit(solution)/shard_map/all_gather | solution.py:125
  230.6 6.9 %copy-start.6 = (f32[64]{0:T(128)S(1)}, f32[64]{0:T(128)}, u32[]{:S(2)}) copy-start(f32[64]{0:T(128)} %param.13) | copy-start | bytes 772
  232.6 29.9 %all-to-all-start.4 = ((bf16[2,512,512]{2,0,1:T(2,128)(2,1)}), bf16[2,512,512]{2,0,1:T(2,128)(2,1)S(1)}, u32[]{:S(2)}, u32[]{:S(2)}) async-start(bf16[2,512,512]{2,0,1:T(2,128)(2,1)} %copy.77), calls=%async_computation.4 | async-start | bytes 2097152 | tf_op jit(solution)/shard_map/all_to_all | solution.py:68
  242.0 26.2 %copy-start.1 = (f32[64,128]{1,0:T(8,128)S(1)}, f32[64,128]{1,0:T(8,128)}, u32[]{:S(2)}) copy-start(f32[64,128]{1,0:T(8,128)} %param.17) | copy-start | bytes 98308
  242.0 26.2 %copy-start.2 = (f32[64,128]{1,0:T(8,128)S(1)}, f32[64,128]{1,0:T(8,128)}, u32[]{:S(2)}) copy-start(f32[64,128]{1,0:T(8,128)} %param.18) | copy-start | bytes 98308
  262.5 111.6 %all-to-all-start = ((bf16[64,64,256]{2,1,0:T(8,128)(2,1)}), bf16[64,64,256]{2,1,0:T(8,128)(2,1)}, u32[]{:S(2)}, u32[]{:S(2)}) async-start(bf16[64,64,256]{2,1,0:T(8,128)(2,1)} %pad_maximum_fusion), calls=%async_computation | async-start | bytes 4194304 | tf_op jit(solution)/shard_map/all_to_all | solution.py:10
  268.1 175.8 %all-gather.5.cloned.1.call-start = ((), (), s32[]{:S(2)}) async-start(), calls=%async_computation.11 | async-start | bytes 1081344 | tf_op jit(solution)/shard_map/all_gather | solution.py:20
  269.0 211.0 %reduce-scatter.2.cloned.1.call-start = ((), (), s32[]{:S(2)}) async-start(), calls=%async_computation.10 | async-start | bytes 9175040 | tf_op jit(solution)/shard_map/reduce_scatter | solution.py:134
  395.8 0.8 copy-start.3
  446.0 0.8 copy-start
  449.5 35.1 %all-to-all-start.7 = ((bf16[4,224,512]{2,1,0:T(8,128)(2,1)}), bf16[4,224,512]{2,1,0:T(8,128)(2,1)S(1)}, u32[]{:S(2)}, u32[]{:S(2)}) async-start(bf16[4,224,512]{2,1,0:T(8,128)(2,1)} %bitcast.73), calls=%async_computation.8 | async-start | bytes 1835008 | tf_op jit(solution)/shard_map/all_to_all | solution.py:47
  484.6 13.3 %copy-start.5 = (f32[224,6]{0,1:T(8,128)S(1)}, f32[224,6]{0,1:T(8,128)}, u32[]{:S(2)}) copy-start(f32[224,6]{0,1:T(8,128)} %param.12) | copy-start | bytes 16132
  484.6 102.0 %all-to-all-start.5 = ((bf16[32,2,28,512]{3,1,2,0:T(2,128)(2,1)}), bf16[32,2,28,512]{3,1,2,0:T(2,128)(2,1)}, u32[]{:S(2)}, u32[]{:S(2)}) async-start(bf16[32,2,28,512]{3,1,2,0:T(2,128)(2,1)} %copy.80), calls=%async_computation.6 | async-start | bytes 3670016 | tf_op jit(solution)/shard_map/all_to_all | solution.py:137
Sparse Core Ops, SparseCore 0:
  176.1 91.4 all-gather.2
  271.4 91.1 all-gather.4
  396.0 83.9 reduce-scatter.1
where the time goes:
time: 612 us; the launch traced here: 608 us
  waiting for transfers between devices  373 us (61%)
  starting transfers between devices  64.3 us (11%)
  local copies, waits for them, and re-layouts  60.1 us (10%)
  blocking collectives  47 us (8%)
  other arithmetic  28.6 us (5%)
  matrix products  21 us (3%)
  between operations  14.1 us (2%)
    all_to_all x1, waiting for transfers between devices, in_one_piece(): lax.all_to_all(both, axis, split_axis=split_dim, concat_axis=concat_dim,...  101 us
    all_to_all x1, waiting for transfers between devices, per_device(): lax.all_to_all(summed, 'fs', split_axis=0, concat_axis=0, tiled=True)  86.3 us
    all_to_all x1, waiting for transfers between devices, per_device(): lax.all_to_all(send_rows, 'fs', split_axis=0, concat_axis=0, tiled=True)  85.9 us
    all_to_all x1, waiting for transfers between devices, per_device(): lax.all_to_all(down_cast, 'fs', split_axis=0, concat_axis=1, tiled=True)  53.7 us
    all_gather x1, blocking collectives, per_device(): lax.all_gather(shared_down_cast, 'fs', axis=0, tiled=True)  28.3 us
    reduce_scatter x1, waiting for transfers between devices, per_device(): lax.psum_scatter(partial_rows.astype(jnp.bfloat16), 'tp', scatter_dimensi...  24.8 us
    all_to_all x1, starting transfers between devices, sent_to_all(): lax.all_to_all(jnp.broadcast_to(x[None], (size, *x.shape)), axis, 0, 0, t...  22.6 us
    all_to_all x1, waiting for transfers between devices, per_device(): lax.all_to_all(lax.all_to_all(down_cast, 'fs', split_axis=0, concat_axis=...  20.5 us
  transfers between devices with their start and end apart: 10, of which 6 were waited for; matrix products, arithmetic and copies ran while one was open for 13% of the time, Pallas kernels for 0%

commit v1 on v0

v1 whole, which is shorter than its diff:
```python
import functools

import jax
import jax.numpy as jnp
from jax import lax
from jax.experimental import pallas as pl
from jax.experimental.pallas import tpu as pltpu
from jax.sharding import PartitionSpec as P

MESH = pl.DeviceIdType.MESH
BF = jnp.bfloat16
F32 = jnp.float32
META = 16
SLOTS = 32


def remote(src, dst, send_sem, recv_sem, **where):
    return pltpu.make_async_remote_copy(
        src_ref=src, dst_ref=dst, send_sem=send_sem, recv_sem=recv_sem, device_id=where, device_id_type=MESH
    )


def far_first(count):
    half = count // 2
    order = [half]
    for d in range(1, half):
        order += [half - d, half + d]
    return order + [0]


def places(chips, cols):
    g, f, t = lax.axis_index("grp"), lax.axis_index("fs"), lax.axis_index("tp")
    c = lax.rem(f, 2)
    z = lax.div(f, 2)
    up = lax.rem(z + 1, chips) * 2 + c
    down = lax.rem(z + chips - 1, chips) * 2 + c
    other = f + 1 - 2 * c
    par = lax.rem(g, 2)
    pair = g + 1 - 2 * par
    right, left = lax.rem(t + 1, cols), lax.rem(t + cols - 1, cols)
    return f, t, c, z, up, down, other, par, pair, right, left


def greet(peers):
    barrier = pltpu.get_barrier_semaphore()
    for peer in peers:
        pl.semaphore_signal(barrier, inc=1, device_id=peer, device_id_type=MESH)
    pl.semaphore_wait(barrier, len(peers))


def collect_kernel(
    chips, cols, toks, held, top, blk, gu, x, xs, gw, sg, su, sd, gu2,
    buf, tri, zs, zr, cs, cr, rs, rr, ls, lr, fs_, fr, ys, yr,
):
    f, t, c, z, up, down, other, par, pair, right, left = places(chips, cols)
    half = chips // 2
    order = far_first(chips)
    pos = {r: p for p, r in enumerate(order)}
    rows = blk.shape[0]
    cut = rows // 2
    width = 2 * SLOTS
    span = sg.shape[0] // (2 * chips)
    dspan = sd.shape[0] // (2 * chips)
    lanes = sg.shape[1]
    wide = tri.shape[0]
    greet([{"fs": up}, {"fs": down}, {"fs": other}, {"tp": right}, {"tp": left}, {"grp": pair}])
    sent = []

    def go(copy):
        copy.start()
        sent.append(copy)
        return copy

    plus, minus, sib = {}, {}, {}
    plus[1] = go(remote(blk, buf.at[chips - 1, c], zs.at[0, 0], zr.at[0, 0], fs=up))
    minus[1] = go(remote(blk, buf.at[1, c], zs.at[1, 0], zr.at[1, 0], fs=down))
    sib[0] = go(remote(blk, buf.at[0, c], cs.at[0], cr.at[0], fs=other))
    mine = blk.at[pl.ds(0, toks)]
    last = chips
    to_right, to_left, onward = {}, {}, {}
    to_right[last] = go(remote(mine, xs.at[t], rs.at[last], rr.at[last], tp=right))
    to_left[last] = go(remote(mine, xs.at[t], ls.at[last], lr.at[last], tp=left))
    swap = go(remote(gu, gu2, ys, yr, grp=pair))
    xs[t] = blk[0:toks]
    buf[0, c] = blk[...]
    tri[...] = jnp.where(
        lax.broadcasted_iota(jnp.int32, (wide, wide), 0) < lax.broadcasted_iota(jnp.int32, (wide, wide), 1), 1.0, 0.0
    ).astype(BF)

    def process(r):
        p = pos[r]

        @pl.loop(0, 2)
        def _(cc):
            meta = buf[r, cc, toks : toks + META, :].astype(F32)
            route, hi, lo = meta[0:top, 0:wide], meta[0:top, wide:], meta[top : 2 * top, 0:wide]
            named, his, los = [], [], []
            for j in range(held):
                hit = route == (f * held + j).astype(F32)
                named.append(jnp.sum(jnp.where(hit, 1.0, 0.0), axis=0, keepdims=True))
                his.append(jnp.sum(jnp.where(hit, hi, 0.0), axis=0, keepdims=True))
                los.append(jnp.sum(jnp.where(hit, lo, 0.0), axis=0, keepdims=True))
            stack = jnp.concatenate(named + [jnp.zeros((8 - held, wide), F32)], axis=0)
            rank = jnp.dot(stack.astype(BF), tri[...], preferred_element_type=F32)
            slot = lax.broadcasted_iota(jnp.int32, (SLOTS, wide), 0).astype(F32)
            picks, ghi, glo = [], [], []
            for j in range(held):
                pick = jnp.where(slot == rank[j : j + 1], 1.0, 0.0) * named[j]
                picks.append(pick)
                ghi.append(pick * his[j])
                glo.append(pick * los[j])
            chosen = jnp.concatenate(picks, axis=0).astype(BF)
            gw[p, cc] = jnp.concatenate(ghi + glo, axis=0).astype(BF)
            got = jnp.dot(chosen, buf[r, cc, 0:wide, :], preferred_element_type=F32).astype(BF)
            at = pl.multiple_of(p * width + cc * SLOTS, SLOTS)
            for j in range(held):
                x[t, j, pl.ds(at, SLOTS), :] = got[j * SLOTS : (j + 1) * SLOTS]
            owner = lax.rem(z + r, chips) * 2 + cc
            piece = buf[r, cc, toks + META : toks + META + span // 2, :]
            row = pl.multiple_of(owner * span, span)
            for h in range(2):
                there = pl.ds(pl.multiple_of(row + h * (span // 2), span // 2), span // 2)
                sg[there, :] = piece[:, 2 * h * lanes : (2 * h + 1) * lanes]
                su[there, :] = piece[:, (2 * h + 1) * lanes : (2 * h + 2) * lanes]
            sd[pl.ds(pl.multiple_of(owner * dspan, dspan), dspan), :] = buf[r, cc, toks + META + span // 2 :, :]

    def block(q, p):
        return x.at[q, :, pl.ds(p * width, width), :]

    def send(r):
        p = pos[r]
        to_right[p] = go(remote(block(t, p), block(t, p), rs.at[p], rr.at[p], tp=right))
        to_left[p] = go(remote(block(t, p), block(t, p), ls.at[p], lr.at[p], tp=left))

    def pass_on(p):
        to_right[p].wait_recv()
        to_left[p].wait_recv()
        source, target = (left, right) if p % 2 == 0 else (right, left)
        ref = xs.at[source] if p == last else block(source, p)
        onward[p] = go(remote(ref, ref, fs_.at[p], fr.at[p], tp=target))

    sib[0].wait_recv()
    process(0)
    send(0)
    waiting = [[last, pos[0]]]
    for d in range(1, half + 1):
        plus[d].wait_recv()
        if d < half:
            src, dst = buf.at[chips - d, c], buf.at[chips - d - 1, c]
            if d + 1 == half:
                src, dst = src.at[pl.ds(0, cut)], dst.at[pl.ds(0, cut)]
            plus[d + 1] = go(remote(src, dst, zs.at[0, d], zr.at[0, d], fs=up))
            here = buf.at[chips - d, c]
            sib[chips - d] = go(remote(here, here, cs.at[chips - d], cr.at[chips - d], fs=other))
        minus[d].wait_recv()
        if d < half:
            src, dst = buf.at[d, c], buf.at[d + 1, c]
            if d + 1 == half:
                src, dst = src.at[pl.ds(cut, cut)], dst.at[pl.ds(cut, cut)]
            minus[d + 1] = go(remote(src, dst, zs.at[1, d], zr.at[1, d], fs=down))
        here = buf.at[d, c]
        sib[d] = go(remote(here, here, cs.at[d], cr.at[d], fs=other))
        near = [chips - d, d] if d < half else [half]
        for r in near:
            sib[r].wait_recv()
            process(r)
        for r in near:
            send(r)
        waiting.append([pos[r] for r in near])
        if len(waiting) > 2:
            for p in waiting.pop(0):
                pass_on(p)
    for group in waiting:
        for p in group:
            pass_on(p)
    for p in onward:
        onward[p].wait_recv()
    swap.wait_recv()
    for copy in sent:
        copy.wait_send()


def layer_kernel(
    chips, cols, x, xs, gw, gu, gu2, sg, su, sd, dn, mixed, dn2, od, os,
    act, sact, y, own, ss, sr, ps, pr, ms, mr, rs, rr, ls, lr, fs_, fr, cs, cr, zs, zr, ws, wr, ys, yr,
):
    f, t, c, z, up, down, other, par, pair, right, left = places(chips, cols)
    half = chips // 2
    order = far_first(chips)
    pos = {r: p for p, r in enumerate(order)}
    toks, quarter = mixed.shape
    lanes = sg.shape[1]
    width = 2 * SLOTS
    parts = 4
    per = chips // parts
    tall = per * width
    across = [lax.rem(t + d, cols) for d in range(1, cols)]
    greet([{"fs": up}, {"fs": down}, {"fs": other}, {"grp": pair}] + [{"tp": a} for a in across])
    sent = []

    def go(copy):
        copy.start()
        sent.append(copy)
        return copy

    swap = go(remote(dn, dn2, ys, yr, grp=pair))
    own_lanes = pl.ds(pl.multiple_of(t * lanes, lanes), lanes)

    @pl.loop(0, parts)
    def _(i):
        at = pl.ds(pl.multiple_of(i * tall, tall), tall)
        for j, weights in ((par, gu), (1 - par, gu2)):
            both = jnp.zeros((tall, 2 * lanes), F32)
            for q in range(cols):
                both += jnp.dot(x[q, j, at, :], weights[q * quarter : (q + 1) * quarter, :], preferred_element_type=F32)
            act[j, at, own_lanes] = (jax.nn.silu(both[:, :lanes]) * both[:, lanes:]).astype(BF)

    to_right, to_left, onward = {}, {}, {}

    def piece(q, i):
        cols_of = pl.ds(pl.multiple_of(q * lanes, lanes), lanes)
        return sact.at[:, cols_of] if i == parts else act.at[:, pl.ds(i * tall, tall), cols_of]

    def send(i):
        to_right[i] = go(remote(piece(t, i), piece(t, i), rs.at[i], rr.at[i], tp=right))
        to_left[i] = go(remote(piece(t, i), piece(t, i), ls.at[i], lr.at[i], tp=left))

    def pass_on(i):
        to_right[i].wait_recv()
        to_left[i].wait_recv()
        source, target = (left, right) if i % 2 == 0 else (right, left)
        onward[i] = go(remote(piece(source, i), piece(source, i), fs_.at[i], fr.at[i], tp=target))

    for i in range(parts):
        send(i)
    sgate = jnp.zeros((toks, lanes), F32)
    sup = jnp.zeros((toks, lanes), F32)
    for q in range(cols):
        there = slice(q * quarter, (q + 1) * quarter)
        sgate += jnp.dot(xs[q], sg[there, :], preferred_element_type=F32)
        sup += jnp.dot(xs[q], su[there, :], preferred_element_type=F32)
    sact[:, own_lanes] = (jax.nn.silu(sgate) * sup).astype(BF)
    send(parts)
    placed = []

    def place(kind, source, target):
        home = pl.ds(pl.multiple_of(t * quarter, quarter), quarter)
        for k, a in enumerate(across):
            rows_of = pl.ds(pl.multiple_of(a * lanes, lanes), lanes)
            placed.append(go(remote(source.at[rows_of, :], target.at[:, home], ws.at[kind, k], wr.at[kind, k], tp=a)))
        target[:, home] = source[pl.ds(pl.multiple_of(t * lanes, lanes), lanes), :]

    pass_on(0)
    pass_on(1)
    swap.wait_recv()
    sibs = {}

    def chunk(i):
        onward[i].wait_recv()
        for j, weights in ((par, dn), (1 - par, dn2)):
            y[j] = jnp.dot(act[j, i * tall : (i + 1) * tall, :], weights[...], preferred_element_type=F32).astype(BF)

        def combine(p, u, cc):
            at = pl.ds(pl.multiple_of(u * width + cc * SLOTS, SLOTS), SLOTS)
            found = jnp.concatenate([y[0, at, :], y[1, at, :]], axis=0)
            twice = jnp.concatenate([found, found], axis=0)
            whole = lax.dot_general(gw[p, cc], twice, (((0,), (0,)), ((), ())), preferred_element_type=F32)
            return whole[0:toks]

        for u in range(per):
            p = i * per + u
            ss[p] = combine(p, u, 1 - c).astype(BF)
            own[p] = combine(p, u, c)
            sibs[p] = go(remote(ss.at[p], sr.at[p], cs.at[p], cr.at[p], fs=other))

    plus, minus = {}, {}
    cut = toks // 2

    def local(r):
        p = pos[r]
        sibs[p].wait_recv()
        return own[p] + sr[p].astype(F32)

    def step(k):
        if k == 0:
            both = local(half)
            ps[0, 0:cut] = both[0:cut].astype(BF)
            ms[0, cut:] = both[cut:].astype(BF)
            low, high = pl.ds(0, cut), pl.ds(cut, cut)
            plus[0] = go(remote(ps.at[0, low], pr.at[0, low], zs.at[0, 0], zr.at[0, 0], fs=up))
            minus[0] = go(remote(ms.at[0, high], mr.at[0, high], zs.at[1, 0], zr.at[1, 0], fs=down))
            return
        ahead, behind = local(half - k), local(half + k)
        plus[k - 1].wait_recv()
        if k == 1:
            ps[1, 0:cut] = (ahead[0:cut] + pr[0, 0:cut].astype(F32)).astype(BF)
            ps[1, cut:] = ahead[cut:].astype(BF)
        else:
            ps[k] = (ahead + pr[k - 1].astype(F32)).astype(BF)
        plus[k] = go(remote(ps.at[k], pr.at[k], zs.at[0, k], zr.at[0, k], fs=up))
        minus[k - 1].wait_recv()
        if k == 1:
            ms[1, 0:cut] = behind[0:cut].astype(BF)
            ms[1, cut:] = (behind[cut:] + mr[0, cut:].astype(F32)).astype(BF)
        else:
            ms[k] = (behind + mr[k - 1].astype(F32)).astype(BF)
        minus[k] = go(remote(ms.at[k], mr.at[k], zs.at[1, k], zr.at[1, k], fs=down))

    done = 0
    for i in range(parts):
        if i + 2 <= parts:
            pass_on(i + 2)
        chunk(i)
        if i == 0:
            place(0, dn, od.at[par])
            place(1, dn2, od.at[1 - par])
            place(2, sd, os)
        while done < half and max(pos[half - done], pos[(half + done) % chips]) < (i + 1) * per and done <= 2 * i:
            step(done)
            done += 1
    onward[parts].wait_recv()
    shared = jnp.dot(sact[...], sd[...], preferred_element_type=F32)
    while done < half:
        step(done)
        done += 1
    total = local(0) + shared
    plus[half - 1].wait_recv()
    minus[half - 1].wait_recv()
    total = total + pr[half - 1].astype(F32) + mr[half - 1].astype(F32)
    mixed[...] = total.astype(BF)
    for copy in placed:
        copy.wait_recv()
    for copy in sent:
        copy.wait_send()


VM = pl.BlockSpec(memory_space=pltpu.VMEM)


def shape(*dims, kind=BF):
    return jax.ShapeDtypeStruct(dims, kind)


def per_device(
    tokens, routes, route_weights, norm_gain, gate_experts, up_experts, down_experts, shared_gate, shared_up, shared_down
):
    fs_count, cols = lax.axis_size("fs"), lax.axis_size("tp")
    chips = fs_count // 2
    par = lax.rem(lax.axis_index("grp"), 2)
    experts, span, lanes = gate_experts.shape
    held = experts // fs_count
    toks, quarter = tokens.shape
    top = routes.shape[1]
    dspan = down_experts.shape[1]
    wide = quarter // 2

    def half_of(w):
        return lax.dynamic_index_in_dim(w.reshape(fs_count, held, *w.shape[1:]), par, 1, keepdims=False)

    gain = norm_gain[None, :, None]
    gu_cast = jnp.concatenate([half_of(gate_experts) * gain, half_of(up_experts) * gain], axis=2).astype(BF)
    gu = lax.all_to_all(gu_cast, "fs", 0, 0, tiled=True).reshape(fs_count * span, 2 * lanes)
    dn = lax.all_to_all(half_of(down_experts).astype(BF), "fs", 0, 0, tiled=True).reshape(fs_count * dspan, quarter)

    widened = tokens.astype(F32)
    mean = lax.psum(jnp.sum(widened * widened, axis=1, keepdims=True), "tp") / (quarter * cols)
    normed = (widened * lax.rsqrt(mean + 1e-06)).astype(BF)
    pad = ((0, 0), (0, wide - toks))
    route = jnp.pad(routes.T.astype(F32), pad, constant_values=-1.0)
    weight = jnp.pad(route_weights.T, pad)
    high = lax.reduce_precision(weight, 8, 7)
    low = weight - high
    meta = jnp.concatenate(
        [
            jnp.concatenate([route, high], axis=1),
            jnp.concatenate([low, jnp.zeros_like(low)], axis=1),
            jnp.zeros((META - 2 * top, quarter), F32),
        ],
        axis=0,
    ).astype(BF)
    sgu = jnp.concatenate([shared_gate * norm_gain[:, None], shared_up * norm_gain[:, None]], axis=1).astype(BF)
    sgu = jnp.concatenate([sgu[: span // 2], sgu[span // 2 :]], axis=1)
    blk = jnp.concatenate([normed, meta, sgu, shared_down.astype(BF)], axis=0)

    dma = pltpu.SemaphoreType.DMA
    slots = chips * 2 * SLOTS
    half = chips // 2
    x, xs, gw, sg, su, sd, gu2 = pl.pallas_call(
        functools.partial(collect_kernel, chips, cols, toks, held, top),
        out_shape=(
            shape(cols, held, slots, quarter), shape(cols, toks, quarter), shape(chips, 2, 4 * SLOTS, wide),
            shape(fs_count * span, lanes), shape(fs_count * span, lanes), shape(fs_count * dspan, quarter),
            shape(*gu.shape),
        ),
        in_specs=[VM] * 2,
        out_specs=(VM,) * 7,
        scratch_shapes=[
            pltpu.VMEM((chips, 2, *blk.shape), BF), pltpu.VMEM((wide, wide), BF),
            dma((2, half)), dma((2, half)), dma((chips,)), dma((chips,)),
            dma((chips + 1,)), dma((chips + 1,)), dma((chips + 1,)), dma((chips + 1,)), dma((chips + 1,)), dma((chips + 1,)),
            dma, dma,
        ],
        compiler_params=pltpu.CompilerParams(collective_id=1, has_side_effects=True, vmem_limit_bytes=48 * 2**20),
        cost_estimate=pl.CostEstimate(flops=60_000_000_000, bytes_accessed=16_000_000, transcendentals=0),
    )(blk, gu)

    parts = 4
    mixed, dn2, od, os = pl.pallas_call(
        functools.partial(layer_kernel, chips, cols),
        out_shape=(
            shape(toks, quarter), shape(*dn.shape), shape(held, lanes, quarter * cols), shape(lanes, quarter * cols),
        ),
        in_specs=[VM] * 9,
        out_specs=(VM,) * 4,
        scratch_shapes=[
            pltpu.VMEM((held, slots, lanes * cols), BF), pltpu.VMEM((toks, lanes * cols), BF),
            pltpu.VMEM((held, slots // parts, quarter), BF), pltpu.VMEM((chips, toks, quarter), F32),
            pltpu.VMEM((chips, toks, quarter), BF), pltpu.VMEM((chips, toks, quarter), BF),
            pltpu.VMEM((half, toks, quarter), BF), pltpu.VMEM((half, toks, quarter), BF),
            pltpu.VMEM((half, toks, quarter), BF), pltpu.VMEM((half, toks, quarter), BF),
            dma((parts + 1,)), dma((parts + 1,)), dma((parts + 1,)), dma((parts + 1,)), dma((parts + 1,)), dma((parts + 1,)),
            dma((chips,)), dma((chips,)), dma((2, half)), dma((2, half)), dma((3, cols - 1)), dma((3, cols - 1)),
            dma, dma,
        ],
        compiler_params=pltpu.CompilerParams(collective_id=2, has_side_effects=True, vmem_limit_bytes=58 * 2**20),
        cost_estimate=pl.CostEstimate(flops=40_000_000_000, bytes_accessed=16_000_000, transcendentals=0),
    )(x, xs, gw, gu, gu2, sg, su, sd, dn)

    first, second = jnp.where(par == 0, gu, gu2), jnp.where(par == 0, gu2, gu)
    gate_ready = jnp.stack([first[:, :lanes], second[:, :lanes]])
    up_ready = jnp.stack([first[:, lanes:], second[:, lanes:]])
    return mixed, gate_ready, up_ready, od, sg, su, os


def solution(mesh):
    return jax.shard_map(
        per_device,
        mesh=mesh,
        in_specs=(
            P(("grp", "fs"), "tp"), P(("grp", "fs"), None), P(("grp", "fs"), None), P("fs"),
            P(None, "fs", "tp"), P(None, "fs", "tp"), P(None, "fs", "tp"),
            P("fs", "tp"), P("fs", "tp"), P("fs", "tp"),
        ),
        out_specs=(
            P(("grp", "fs"), "tp"), P(("grp", "fs"), None, "tp"), P(("grp", "fs"), None, "tp"),
            P(("grp", "fs"), "tp", None), P("grp", "tp"), P("grp", "tp"), P(("grp", "tp"), None),
        ),
        check_vma=False,
    )
```

time: 612 us -> 302 us (0.49)
  waiting for transfers between devices: 373 us -> 44.6 us
  Pallas kernels: 0 us -> 198 us
  local copies, waits for them, and re-layouts: 60.1 us -> 10.8 us
  blocking collectives: 47 us -> 7.52 us
  starting transfers between devices: 64.3 us -> 30.2 us
  other arithmetic: 28.6 us -> 6.54 us
  matrix products: 21 us -> 0 us
  between operations: 14.1 us -> 0.93 us
    all_to_all x7 -> x2, waiting for transfers between devices: 348 us -> 44.6 us  [the longest x1 44.6 us: per_device(): lax.all_to_all(gu_cast, 'fs', 0, 0, tiled=True)]
    pallas_call x0 -> x2, Pallas kernels: none -> 198 us  [the longest x1 113 us: per_device(): pl.pallas_call(functools.partial(collect_kernel, chips, cols, toks, held,...]
    all_to_all x7 -> x2, starting transfers between devices: 64.1 us -> 30.2 us  [the longest x1 24.7 us: per_device(): lax.all_to_all(gu_cast, 'fs', 0, 0, tiled=True)]
    all_gather x1 -> x0, blocking collectives: 28.3 us -> none  [per_device(): lax.all_gather(shared_down_cast, 'fs', axis=0, tiled=True)]
    reduce_scatter x1 -> x0, waiting for transfers between devices: 24.8 us -> none  [per_device(): lax.psum_scatter(partial_rows.astype(jnp.bfloat16), 'tp', scatter_dimensi...]
    dot_general x5 -> x0, matrix products: 21 us -> none  [the longest x1 11.9 us: per_device(): jnp.einsum('sjcf,jfd->sjcd', active, down_local, preferred_element_type=j...]
    all_to_all x1 -> x0, blocking collectives: 18.7 us -> none  [per_device(): lax.all_to_all(shared_down_rows, 'tp', split_axis=0, concat_axis=1, tiled...]
    all_to_all x10 -> x0, local copies, waits for them, and re-layouts: 15.4 us -> none  [the longest x4 4.87 us: per_device(): lax.all_to_all(lax.all_to_all(down_cast, 'fs', split_axis=0, concat_axis=...]
  transfers between devices with their start and end apart: 10 -> 2, of which waited for: 6 -> 1; matrix products, arithmetic and copies ran while one was open for 13% -> 1% of each run, Pallas kernels for 0% -> 38%
where the time goes in v1:
time: 302 us; the launch traced here: 298 us
  Pallas kernels  198 us (66%)
  waiting for transfers between devices  44.6 us (15%)
  starting transfers between devices  30.2 us (10%)
  local copies, waits for them, and re-layouts  10.8 us (4%)
  blocking collectives  7.52 us (2%)
  other arithmetic  6.54 us (2%)
    pallas_call x1, Pallas kernels, per_device(): pl.pallas_call(functools.partial(collect_kernel, chips, cols, toks, held,...  113 us
    pallas_call x1, Pallas kernels, per_device(): pl.pallas_call(functools.partial(layer_kernel, chips, cols), out_shape=(s...  85.3 us
    all_to_all x1, waiting for transfers between devices, per_device(): lax.all_to_all(gu_cast, 'fs', 0, 0, tiled=True)  44.6 us
    all_to_all x1, starting transfers between devices, per_device(): lax.all_to_all(gu_cast, 'fs', 0, 0, tiled=True)  24.7 us
    unnamed x47, local copies, waits for them, and re-layouts  8.38 us
    psum x1, blocking collectives, per_device(): lax.psum(jnp.sum(widened * widened, axis=1, keepdims=True), 'tp')  7.52 us
  transfers between devices with their start and end apart: 2, of which 1 were waited for; matrix products, arithmetic and copies ran while one was open for 1% of the time, Pallas kernels for 38%

profile of v1, /device:TPU:38, one launch (start us, length us, event | category | flops | bytes accessed | tf_op | source)
XLA Modules:
  0.0 298.3 jit_solution(17885285259197436041)
XLA Ops:
  0.6 0.0 copy-start
  0.7 2.1 fusion.1
  2.7 0.0 copy-start.17
  2.7 0.0 copy-start.19
  2.7 0.0 copy-start.12
  2.8 0.0 copy-start.18
  2.8 0.0 copy-start.15
  2.8 0.0 copy-start.16
  2.8 0.0 copy-start.20
  2.8 1.1 pad_maximum_fusion
  3.9 24.7 %all-to-all-start = ((bf16[32,64,256]{2,1,0:T(8,128)(2,1)}), bf16[32,64,256]{2,1,0:T(8,128)(2,1)S(1)}, u32[]{:S(2)}, u32[]{:S(2)}) async-start(bf16[32,64,256]{2,1,0:T(8,128)(2,1)} %pad_maximum_fusion), calls=%async_computation | async-start | bytes 2097152 | tf_op jit(solution)/shard_map/all_to_all | solution.py:362
  28.7 0.0 copy-done.17
  28.7 0.0 copy-done.19
  28.7 0.0 copy-done.12
  28.8 0.1 fusion.3
  28.9 7.5 %psum.7 = f32[224,1]{0,1:T(1,128)S(1)} all-reduce(f32[224,1]{0,1:T(1,128)S(1)} %bitcast.41), channel_id=1, replica_groups=mesh['grp'=2,'fs'=32,'tp'=4] {'tp'}, use_global_device_ids=true, to_apply=%region_1.2 | all-reduce | flops 224 | bytes 1792 | tf_op jit(solution)/shard_map/psum | solution.py:366
  36.4 0.0 copy-done.18
  36.4 0.0 copy-done.15
  36.4 0.0 copy-done.16
  36.4 0.0 copy-done.20
  36.4 0.1 multiply_convert_fusion.1
  36.6 0.8 fusion.4
  37.4 1.1 concatenate.28.blk
  38.4 0.0 copy-done
  38.4 0.9 fusion.2
  39.4 44.6 %all-to-all-done = bf16[32,64,256]{2,1,0:T(8,128)(2,1)S(1)} async-done(((bf16[32,64,256]{2,1,0:T(8,128)(2,1)}), bf16[32,64,256]{2,1,0:T(8,128)(2,1)S(1)}, u32[]{:S(2)}, u32[]{:S(2)}) %all-to-all-start) | async-done | bytes 1048608 | tf_op jit(solution)/shard_map/all_to_all | solution.py:362
  84.0 0.0 copy-start.1
  84.0 5.4 %all-to-all-start.1 = ((bf16[32,16,512]{2,1,0:T(8,128)(2,1)}), bf16[32,16,512]{2,1,0:T(8,128)(2,1)}, u32[]{:S(2)}, u32[]{:S(2)}) async-start(bf16[32,16,512]{2,1,0:T(8,128)(2,1)} %fusion.2), calls=%async_computation.1 | async-start | bytes 1048576 | tf_op jit(solution)/shard_map/all_to_all | solution.py:363
  89.4 112.5 %shard_map.153 = (bf16[4,2,1024,512]{3,2,1,0:T(8,128)(2,1)}, bf16[4,224,512]{2,1,0:T(8,128)(2,1)S(1)}, bf16[16,2,128,256]{3,2,1,0:T(8,128)(2,1)}, bf16[2048,128]...) custom-call(bf16[288,512]{1,0:T(8,128)(2,1)S(1)} %concatenate.28.blk, ...), custom_call_target="tpu_custom_call" | custom-call | flops 60000002048 | bytes 16000000 | tf_op jit(solution)/shard_map/pallas_call | solution.py:388
  201.9 0.0 copy-done.1
  201.9 0.0 copy-start.3
  201.9 1.0 copy-done.3
  202.9 0.0 copy-start.5
  202.9 0.8 copy-done.5
  203.7 0.0 copy-start.7
  203.7 0.8 copy-done.7
  204.5 0.0 copy-start.9
  204.5 0.9 copy-done.9
  205.4 0.0 copy-start.10
  205.4 0.8 copy-done.10
  206.2 0.0 all-to-all-done.1
  206.2 0.0 copy-start.2
  206.2 0.0 copy-start.4
  206.2 85.3 %shard_map.154 = (bf16[224,512]{1,0:T(8,128)(2,1)}, bf16[512,512]{1,0:T(8,128)(2,1)}, bf16[2,128,2048]{2,1,0:T(8,128)(2,1)}, bf16[128,2048]{1,0:T(8,128)(2,1)}) custom-call(bf16[4,2,1024,512]{3,2,1,0:T(8,128)(2,1)} %get-tuple-element.17.x, bf16[4,224,512]{2,1,0:T(8,128)(2,1)} %copy-done.9, bf16[16,2,128,256]{3,2,1,0:T(8,128)(2,1)} %get-tuple-element.19.gw, ...), custom_call_target="tpu_custom_call" | custom-call | flops 40000000000 | bytes 16000000 | tf_op jit(solution)/shard_map/pallas_call | solution.py:408
  291.5 0.0 copy-done.2
  291.5 0.0 copy-done.4
  291.5 0.2 broadcast_select_fusion.1
  291.7 0.4 slice_bitcast_fusion
  292.1 0.0 copy-start.14
  292.1 0.0 copy-start.11
  292.1 1.1 pad_maximum_fusion.2
  293.2 0.0 copy-start.8
  293.2 1.1 pad_maximum_fusion.1
  294.2 0.0 copy-done.14
  294.2 0.0 copy-start.6
  294.2 0.7 copy.25
  294.9 0.0 copy-done.11
  294.9 1.0 copy.26
  295.9 0.0 copy-done.8
  295.9 0.8 copy.27
  296.7 0.0 copy-done.6
  296.7 0.8 copy.28
  297.5 0.0 copy-done.13
  297.5 0.8 copy.29
  (10 shorter events, 0.1 us)
Async XLA Ops:
  0.6 37.8 %copy-start = (f32[64,16,512]{2,1,0:T(8,128)S(1)}, f32[64,16,512]{2,1,0:T(8,128)}, u32[]{:S(2)}) copy-start(f32[64,16,512]{2,1,0:T(8,128)} %param.16) | copy-start | bytes 6291460
  2.7 26.0 %copy-start.17 = (f32[16,512]{1,0:T(8,128)S(1)}, f32[16,512]{1,0:T(8,128)}, u32[]{:S(2)}) copy-start(f32[16,512]{1,0:T(8,128)} %param.19) | copy-start | bytes 98308
  2.7 26.0 %copy-start.19 = (f32[224,6]{0,1:T(8,128)S(1)}, f32[224,6]{0,1:T(8,128)}, u32[]{:S(2)}) copy-start(f32[224,6]{0,1:T(8,128)} %param.12) | copy-start | bytes 16132
  2.7 26.0 %copy-start.12 = (bf16[224,512]{1,0:T(8,128)(2,1)S(1)}, bf16[224,512]{1,0:T(8,128)(2,1)}, u32[]{:S(2)}) copy-start(bf16[224,512]{1,0:T(8,128)(2,1)} %param.10) | copy-start | bytes 688132
  2.8 33.6 %copy-start.18 = (s32[224,6]{0,1:T(8,128)S(1)}, s32[224,6]{0,1:T(8,128)}, u32[]{:S(2)}) copy-start(s32[224,6]{0,1:T(8,128)} %param.11) | copy-start | bytes 16132
  2.8 33.6 %copy-start.15 = (f32[64,128]{1,0:T(8,128)S(1)}, f32[64,128]{1,0:T(8,128)}, u32[]{:S(2)}) copy-start(f32[64,128]{1,0:T(8,128)} %param.17) | copy-start | bytes 98308
  2.8 33.6 %copy-start.16 = (f32[64,128]{1,0:T(8,128)S(1)}, f32[64,128]{1,0:T(8,128)}, u32[]{:S(2)}) copy-start(f32[64,128]{1,0:T(8,128)} %param.18) | copy-start | bytes 98308
  2.8 33.6 %copy-start.20 = (f32[64]{0:T(128)S(1)}, f32[64]{0:T(128)}, u32[]{:S(2)}) copy-start(f32[64]{0:T(128)} %param.13) | copy-start | bytes 772
  3.9 80.1 %all-to-all-start = ((bf16[32,64,256]{2,1,0:T(8,128)(2,1)}), bf16[32,64,256]{2,1,0:T(8,128)(2,1)S(1)}, u32[]{:S(2)}, u32[]{:S(2)}) async-start(bf16[32,64,256]{2,1,0:T(8,128)(2,1)} %pad_maximum_fusion), calls=%async_computation | async-start | bytes 2097152 | tf_op jit(solution)/shard_map/all_to_all | solution.py:362
  84.0 118.0 %copy-start.1 = (bf16[32,64,256]{2,1,0:T(8,128)(2,1)}, bf16[32,64,256]{2,1,0:T(8,128)(2,1)S(1)}, u32[]{:S(2)}) copy-start(bf16[32,64,256]{2,1,0:T(8,128)(2,1)S(1)} %all-to-all-done) | copy-start | bytes 3145732
  84.0 122.2 %all-to-all-start.1 = ((bf16[32,16,512]{2,1,0:T(8,128)(2,1)}), bf16[32,16,512]{2,1,0:T(8,128)(2,1)}, u32[]{:S(2)}, u32[]{:S(2)}) async-start(bf16[32,16,512]{2,1,0:T(8,128)(2,1)} %fusion.2), calls=%async_computation.1 | async-start | bytes 1048576 | tf_op jit(solution)/shard_map/all_to_all | solution.py:363
  201.9 1.0 copy-start.3
  202.9 0.8 copy-start.5
  203.7 0.8 copy-start.7
  204.5 0.9 copy-start.9
  205.4 0.8 copy-start.10
  206.2 85.3 %copy-start.2 = (bf16[32,64,256]{2,1,0:T(8,128)(2,1)S(1)}, bf16[32,64,256]{2,1,0:T(8,128)(2,1)}, u32[]{:S(2)}) copy-start(bf16[32,64,256]{2,1,0:T(8,128)(2,1)} %copy-done.1) | copy-start | bytes 3145732
  206.2 85.3 %copy-start.4 = (bf16[2048,256]{1,0:T(8,128)(2,1)S(1)}, bf16[2048,256]{1,0:T(8,128)(2,1)}, u32[]{:S(2)}) copy-start(bf16[2048,256]{1,0:T(8,128)(2,1)} %copy-done.3) | copy-start | bytes 3145732
  292.1 2.1 copy-start.14
  292.1 2.8 copy-start.11
  293.2 2.7 copy-start.8
  294.2 2.5 copy-start.6
  294.9 2.6 copy-start.13

commit v2 on v1

v2 whole, which is shorter than its diff:
```python
import functools

import jax
import jax.numpy as jnp
from jax import lax
from jax.experimental import pallas as pl
from jax.experimental.pallas import tpu as pltpu
from jax.sharding import PartitionSpec as P

MESH = pl.DeviceIdType.MESH
BF = jnp.bfloat16
F32 = jnp.float32
META = 16
SLOTS = 32


def remote(src, dst, send_sem, recv_sem, **where):
    return pltpu.make_async_remote_copy(
        src_ref=src, dst_ref=dst, send_sem=send_sem, recv_sem=recv_sem, device_id=where, device_id_type=MESH
    )


def far_first(count):
    half = count // 2
    order = [half]
    for d in range(1, half):
        order += [half - d, half + d]
    return order + [0]


def places(chips, cols):
    g, f, t = lax.axis_index("grp"), lax.axis_index("fs"), lax.axis_index("tp")
    c = lax.rem(f, 2)
    z = lax.div(f, 2)
    up = lax.rem(z + 1, chips) * 2 + c
    down = lax.rem(z + chips - 1, chips) * 2 + c
    other = f + 1 - 2 * c
    par = lax.rem(g, 2)
    pair = g + 1 - 2 * par
    right, left = lax.rem(t + 1, cols), lax.rem(t + cols - 1, cols)
    return f, t, c, z, up, down, other, par, pair, right, left


def greet(peers):
    barrier = pltpu.get_barrier_semaphore()
    for peer in peers:
        pl.semaphore_signal(barrier, inc=1, device_id=peer, device_id_type=MESH)

    def answered():
        pl.semaphore_wait(barrier, len(peers))

    return answered


def whole_kernel(
    chips, cols, held, top,
    tok, routes, weights_of, gain, sgate_own, sup_own, sdown_own, gates, ups, downs,
    mixed, gate_out, up_out, od_out, os_out, sg_out, su_out,
    gf, uf, df, gcast, dcast, table, gu, gu2, od, os, sg, su, in_sem, out_sem, raw, xn, buf, tri, x, gw, sd, dn, dn2, act, sact, y, own, ss, sr, ps, pr, ms, mr,
    gs, gr, ds_, dr, gys, gyr, dys, dyr, ts, tr, zs, zr, cs, cr, rs, rr, ls, lr, fs_, fr,
    ars, arr, als, alr, afs, afr, bs, br, vs, vr, ws, wr,
):
    f, t, c, z, up, down, other, par, pair, right, left = places(chips, cols)
    fs_count = 2 * chips
    half = chips // 2
    order = far_first(chips)
    pos = {r: p for p, r in enumerate(order)}
    toks, quarter = tok.shape
    lanes = sg.shape[1]
    rows = buf.shape[2]
    cut = rows // 2
    width = 2 * SLOTS
    wide = tri.shape[0]
    span, dspan = gcast.shape[1], dcast.shape[1]
    parts = 4
    per = chips // parts
    tall = per * width
    tcut = toks // 2
    across = [lax.rem(t + d, cols) for d in range(1, cols)]

    def core(delta, k):
        return lax.rem(z + delta, chips) * 2 + k

    away = [(delta, k) for delta in range(1, chips) for k in range(2)]
    fetched = [
        pltpu.make_async_copy(src.at[:, par], dst, in_sem.at[n])
        for n, (src, dst) in enumerate(((gates, gf), (ups, uf), (downs, df)))
    ]
    for copy in fetched:
        copy.start()
    answered = greet(
        [{"fs": core(delta, k)} for delta, k in away]
        + [{"fs": other}, {"grp": pair}]
        + [{"tp": a} for a in across]
    )
    sent = []

    def go(copy):
        copy.start()
        sent.append(copy)
        return copy

    def part(ref, owner, size, count=1):
        return ref.at[pl.ds(pl.multiple_of(owner * size, size), count * size), :]

    def hand(cast, target, size, sends, recvs, delta, k):
        there = core(delta, k)
        back = (chips - delta) % chips
        go(remote(cast.at[there], part(target, f, size), sends.at[delta, k], recvs.at[back, c], fs=there))

    def landed(target, size, sends, recvs, delta, k):
        here = part(target, core(delta, k), size)
        remote(here, here, sends.at[delta, k], recvs.at[delta, k], fs=core(delta, k)).wait_recv()

    def hand_gates(d):
        for delta in sorted({d, chips - d}):
            for k in range(2):
                hand(gcast, gu, span, gs, gr, delta, k)

    def swap_chip(target, target2, size, sends, recvs, delta):
        here, there = (part(v, core(delta, 0), size, 2) for v in (target, target2))
        return go(remote(here, there, sends.at[delta], recvs.at[delta], grp=pair))

    table[...] = jnp.full(table.shape, -1.0, F32)
    table[0:toks, 0:top] = routes[...].astype(F32)
    table[0:toks, 8 : 8 + top] = weights_of[...]
    turned = table[...].T
    weight = turned[8:16, :]
    high = weight.astype(BF)
    low = (weight - high.astype(F32)).astype(BF)
    short = span // 2
    scaled = [(v[...] * gain[...]).astype(BF) for v in (sgate_own, sup_own)]
    buf[0, c, toks : toks + 8, 0:wide] = turned[0:8, :].astype(BF)
    buf[0, c, toks : toks + 8, wide:] = high
    buf[0, c, toks + 8 : toks + META, 0:wide] = low
    buf[0, c, toks + 8 : toks + META, wide:] = jnp.zeros_like(low)
    for h in range(2):
        for n in range(2):
            at = (2 * h + n) * lanes
            buf[0, c, toks + META : toks + META + short, at : at + lanes] = scaled[n][h * short : (h + 1) * short]
    buf[0, c, toks + META + short :, :] = sdown_own[...].astype(BF)
    for copy in fetched:
        copy.wait()

    @pl.loop(0, fs_count)
    def _(i):
        gcast[i, :, 0:lanes] = (gf[i] * gain[...]).astype(BF)
        gcast[i, :, lanes:] = (uf[i] * gain[...]).astype(BF)
        dcast[i] = df[i].astype(BF)

    answered()
    traded = [
        go(remote(tok, raw.at[t], ts.at[0], tr.at[0], tp=right)),
        go(remote(tok, raw.at[t], ts.at[1], tr.at[1], tp=left)),
    ]
    for d in range(1, half // 2 + 1):
        hand_gates(d)
    go(remote(gcast.at[other], part(gu, f, span), gs.at[0, 0], gr.at[0, 0], fs=other))
    go(remote(dcast.at[other], part(dn, f, dspan), ds_.at[0, 0], dr.at[0, 0], fs=other))
    part(gu, f, span)[...] = gcast[f]
    part(dn, f, dspan)[...] = dcast[f]
    tri[...] = jnp.where(
        lax.broadcasted_iota(jnp.int32, (wide, wide), 0) < lax.broadcasted_iota(jnp.int32, (wide, wide), 1), 1.0, 0.0
    ).astype(BF)
    traded[0].wait_recv()
    upper, lower = pl.ds(0, tcut), pl.ds(tcut, tcut)
    traded.append(go(remote(raw.at[left, upper], raw.at[left, upper], ts.at[2], tr.at[2], tp=right)))
    traded[1].wait_recv()
    traded.append(go(remote(raw.at[right, lower], raw.at[right, lower], ts.at[3], tr.at[3], tp=left)))
    traded[2].wait_recv()
    traded[3].wait_recv()
    opposite = across[cols // 2 - 1]
    sources = [(t, tok)] + [(q, raw.at[q]) for q in (left, right, opposite)]
    total = jnp.zeros((toks, 1), F32)
    for _, ref in sources:
        value = ref[...].astype(F32)
        total += jnp.sum(value * value, axis=1, keepdims=True)
    scale = lax.rsqrt(total / (quarter * cols) + 1e-06)
    buf[0, c, 0:toks, :] = (tok[...].astype(F32) * scale).astype(BF)
    for q, ref in sources:
        xn[q] = (ref[...].astype(F32) * scale).astype(BF)

    def process(r):
        p = pos[r]

        @pl.loop(0, 2)
        def _(cc):
            meta = buf[r, cc, toks : toks + META, :].astype(F32)
            route, hi, lo = meta[0:8, 0:wide], meta[0:8, wide:], meta[8:META, 0:wide]
            named, his, los = [], [], []
            for j in range(held):
                hit = route == (f * held + j).astype(F32)
                named.append(jnp.sum(jnp.where(hit, 1.0, 0.0), axis=0, keepdims=True))
                his.append(jnp.sum(jnp.where(hit, hi, 0.0), axis=0, keepdims=True))
                los.append(jnp.sum(jnp.where(hit, lo, 0.0), axis=0, keepdims=True))
            stack = jnp.concatenate(named + [jnp.zeros((8 - held, wide), F32)], axis=0)
            rank = jnp.dot(stack.astype(BF), tri[...], preferred_element_type=F32)
            slot = lax.broadcasted_iota(jnp.int32, (SLOTS, wide), 0).astype(F32)
            picks, ghi, glo = [], [], []
            for j in range(held):
                pick = jnp.where(slot == rank[j : j + 1], 1.0, 0.0) * named[j]
                picks.append(pick)
                ghi.append(pick * his[j])
                glo.append(pick * los[j])
            chosen = jnp.concatenate(picks, axis=0).astype(BF)
            gw[p, cc] = jnp.concatenate(ghi + glo, axis=0).astype(BF)
            got = jnp.dot(chosen, buf[r, cc, 0:wide, :], preferred_element_type=F32).astype(BF)
            at = pl.multiple_of(p * width + cc * SLOTS, SLOTS)
            for j in range(held):
                x[t, j, pl.ds(at, SLOTS), :] = got[j * SLOTS : (j + 1) * SLOTS]
            owner = lax.rem(z + r, chips) * 2 + cc
            piece = buf[r, cc, toks + META : toks + META + short, :]
            for h in range(2):
                there = pl.ds(pl.multiple_of(owner * span + h * short, short), short)
                sg[there, :] = piece[:, 2 * h * lanes : (2 * h + 1) * lanes]
                su[there, :] = piece[:, (2 * h + 1) * lanes : (2 * h + 2) * lanes]
            sd[pl.ds(pl.multiple_of(owner * dspan, dspan), dspan), :] = buf[r, cc, toks + META + short :, :]

    def block(q, p):
        return x.at[q, :, pl.ds(p * width, width), :]

    to_right, to_left, onward = {}, {}, {}

    def send_rows(r):
        p = pos[r]
        to_right[p] = go(remote(block(t, p), block(t, p), rs.at[p], rr.at[p], tp=right))
        to_left[p] = go(remote(block(t, p), block(t, p), ls.at[p], lr.at[p], tp=left))

    def pass_rows(p):
        to_right[p].wait_recv()
        to_left[p].wait_recv()
        source, target = (left, right) if p % 2 == 0 else (right, left)
        onward[p] = go(remote(block(source, p), block(source, p), fs_.at[p], fr.at[p], tp=target))

    ring, sib = {}, {}
    bounds = [pl.ds(0, cut), pl.ds(cut, cut)]

    def forward(way, h, d):
        step = chips - d if way == 0 else d
        before = (step + 1) % chips if way == 0 else step - 1
        src, dst = buf.at[before, c, bounds[h]], buf.at[step, c, bounds[h]]
        ring[way, h, d] = go(
            remote(src, dst, zs.at[way, h, d - 1], zr.at[way, h, d - 1], fs=up if way == 0 else down)
        )

    def share(r, h):
        here = buf.at[r, c, bounds[h]]
        sib[r, h] = go(remote(here, here, cs.at[r, h], cr.at[r, h], fs=other))

    flows = [(0, 0), (1, 1), (0, 1), (1, 0)]
    for way, h in flows:
        forward(way, h, 1)
    for h in range(2):
        share(0, h)
    waiting = []
    gate_swaps = {}

    def swap_gates(delta):
        for k in range(2):
            landed(gu, span, gs, gr, delta, k)
        gate_swaps[delta] = swap_chip(gu, gu2, span, gys, gyr, delta)

    remote(part(gu, other, span), part(gu, other, span), gs.at[0, 0], gr.at[0, 0], fs=other).wait_recv()
    gate_swaps[0] = swap_chip(gu, gu2, span, gys, gyr, 0)

    def settle(near):
        for r in near:
            for h in range(2):
                sib[r, h].wait_recv()
            process(r)
        for r in near:
            send_rows(r)
        waiting.extend(pos[r] for r in near)

    def swap_ring(d):
        for delta in sorted({d, chips - d}):
            swap_gates(delta)

    def pass_waiting():
        while waiting:
            pass_rows(waiting.pop(0))

    ready = {half // 2: (1,), half // 2 + 1: (2, 3), half - 2: (4,), half - 1: (5,), half: (6,)} if half == 8 else {}

    def hand_downs():
        for d in range(1, half + 1):
            for delta in sorted({d, chips - d}):
                for k in range(2):
                    hand(dcast, dn, dspan, ds_, dr, delta, k)

    settle([0])
    for d in range(1, half + 1):
        for way, h in flows:
            if d == half and way != h:
                continue
            ring[way, h, d].wait_recv()
            if d + 1 < half or (d + 1 == half and way == h):
                forward(way, h, d + 1)
            share(chips - d if way == 0 else d, h)
        later = half // 2 + (d + 1) // 2
        if d % 2 == 1 and later <= half:
            hand_gates(later)
        if d == half - 1:
            hand_downs()
        pass_waiting()
        settle([chips - d, d] if d < half else [half])
        for n in ready.get(d, ()):
            swap_ring(n)
    onward[pos[half]] = go(
        remote(block(t, pos[half]), block(t, pos[half]), fs_.at[pos[half]], fr.at[pos[half]], tp=opposite)
    )
    for n in range(1, half + 1):
        if n not in sum(ready.values(), ()):
            swap_ring(n)
    to_right[pos[half]].wait_recv()
    to_left[pos[half]].wait_recv()
    for p in onward:
        onward[p].wait_recv()
    down_swaps = []

    def land_downs(d):
        for delta in sorted({d, chips - d} if d else {0}):
            if delta:
                for k in range(2):
                    landed(dn, dspan, ds_, dr, delta, k)
            else:
                remote(part(dn, other, dspan), part(dn, other, dspan), ds_.at[0, 0], dr.at[0, 0], fs=other).wait_recv()
            down_swaps.append(swap_chip(dn, dn2, dspan, dys, dyr, delta))

    for d in range(half // 2):
        land_downs(d)

    own_lanes = pl.ds(pl.multiple_of(t * lanes, lanes), lanes)

    def hidden(j, at, weights):
        both = jnp.zeros((tall, 2 * lanes), F32)
        for q in range(cols):
            both += jnp.dot(x[q, j, at, :], weights[q * quarter : (q + 1) * quarter, :], preferred_element_type=F32)
        act[j, at, own_lanes] = (jax.nn.silu(both[:, :lanes]) * both[:, lanes:]).astype(BF)

    @pl.loop(0, parts)
    def _(i):
        hidden(par, pl.ds(pl.multiple_of(i * tall, tall), tall), gu)

    for delta in gate_swaps:
        gate_swaps[delta].wait_recv()
    outs = []

    def leave(src, dst):
        copy = pltpu.make_async_copy(src, dst, out_sem.at[len(outs)])
        copy.start()
        outs.append(copy)

    to_right2, to_left2, onward2 = {}, {}, {}

    def piece(q, i):
        cols_of = pl.ds(pl.multiple_of(q * lanes, lanes), lanes)
        return sact.at[:, cols_of] if i == parts else act.at[:, pl.ds(i * tall, tall), cols_of]

    def send_act(i):
        to_right2[i] = go(remote(piece(t, i), piece(t, i), ars.at[i], arr.at[i], tp=right))
        to_left2[i] = go(remote(piece(t, i), piece(t, i), als.at[i], alr.at[i], tp=left))

    def pass_act(i):
        to_right2[i].wait_recv()
        to_left2[i].wait_recv()
        if i == 0:
            return
        source, target = (left, right) if i % 2 == 0 else (right, left)
        onward2[i] = go(remote(piece(source, i), piece(source, i), afs.at[i], afr.at[i], tp=target))

    for i in range(parts):
        hidden(1 - par, pl.ds(i * tall, tall), gu2)
        send_act(i)
        if i == 0:
            onward2[0] = go(remote(piece(t, 0), piece(t, 0), afs.at[0], afr.at[0], tp=opposite))
    sgate = jnp.zeros((toks, lanes), F32)
    sup = jnp.zeros((toks, lanes), F32)
    for q in range(cols):
        there = slice(q * quarter, (q + 1) * quarter)
        sgate += jnp.dot(xn[q], sg[there, :], preferred_element_type=F32)
        sup += jnp.dot(xn[q], su[there, :], preferred_element_type=F32)
    sact[:, own_lanes] = (jax.nn.silu(sgate) * sup).astype(BF)
    send_act(parts)
    placed = []

    def place(kind, source, target):
        home = pl.ds(pl.multiple_of(t * quarter, quarter), quarter)
        for k, a in enumerate(across):
            rows_of = pl.ds(pl.multiple_of(a * lanes, lanes), lanes)
            placed.append(go(remote(source.at[rows_of, :], target.at[:, home], ws.at[kind, k], wr.at[kind, k], tp=a)))
        target[:, home] = source[pl.ds(pl.multiple_of(t * lanes, lanes), lanes), :]

    land_downs(half // 2)
    land_downs(half // 2 + 1)
    pass_act(0)
    land_downs(half // 2 + 2)
    pass_act(1)
    for d in range(half // 2 + 3, half + 1):
        land_downs(d)
    for copy in down_swaps:
        copy.wait_recv()
    sibs = {}

    def chunk(i):
        onward2[i].wait_recv()
        for j, weights in ((par, dn), (1 - par, dn2)):
            y[j] = jnp.dot(act[j, i * tall : (i + 1) * tall, :], weights[...], preferred_element_type=F32).astype(BF)

        def combine(p, u, cc):
            at = pl.ds(pl.multiple_of(u * width + cc * SLOTS, SLOTS), SLOTS)
            found = jnp.concatenate([y[0, at, :], y[1, at, :]], axis=0)
            twice = jnp.concatenate([found, found], axis=0)
            whole = lax.dot_general(gw[p, cc], twice, (((0,), (0,)), ((), ())), preferred_element_type=F32)
            return whole[0:toks]

        for u in range(per):
            p = i * per + u
            ss[p] = combine(p, u, 1 - c).astype(BF)
            sibs[p] = go(remote(ss.at[p], sr.at[p], bs.at[p], br.at[p], fs=other))
            own[p] = combine(p, u, c)
            if p == 1:
                step(0)

    sums = {}
    limits = [slice(0, tcut), slice(tcut, toks)]
    met = set()

    def local(r, h):
        p = pos[r]
        if p not in met:
            met.add(p)
            sibs[p].wait_recv()
        return own[p, limits[h], :] + sr[p, limits[h], :].astype(F32)

    def add_on(way, h, r):
        out, into = ((ps, pr), (ms, mr))[way]
        k = half - r if way == 0 else r - half
        value = local(r, h)
        first = way != h and k == 1 or k == 0
        if not first:
            sums[way, h, k - 1].wait_recv()
            value = value + into[k - 1, limits[h], :].astype(F32)
        out[k, limits[h], :] = value.astype(BF)
        there = (upper, lower)[h]
        sums[way, h, k] = go(
            remote(out.at[k, there], into.at[k, there], vs.at[way, h, k], vr.at[way, h, k], fs=up if way == 0 else down)
        )

    def step(k):
        for way, h in flows:
            if k == 0 and way != h:
                continue
            add_on(way, h, half - k if way == 0 else half + k)

    done = 1
    for i in range(parts):
        if i + 2 <= parts:
            pass_act(i + 2)
        chunk(i)
        while done < half and max(pos[half - done], pos[(half + done) % chips]) < (i + 1) * per and done <= 2 * i:
            step(done)
            done += 1
        if i == 0:
            place(0, dn, od.at[par])
            place(1, dn2, od.at[1 - par])
            place(2, sd, os)
            for n, (mine, theirs, target) in enumerate(
                ((gu, gu2, gate_out), (gu, gu2, up_out))
            ):
                these = pl.ds(n * lanes, lanes)
                leave(mine.at[:, these], target.at[par])
                leave(theirs.at[:, these], target.at[1 - par])
            leave(sg, sg_out)
            leave(su, su_out)
    onward2[parts].wait_recv()
    shared = jnp.dot(sact[...], sd[...], preferred_element_type=F32)
    own[pos[0]] = own[pos[0]] + shared
    while done < half:
        step(done)
        done += 1
    for copy in placed:
        copy.wait_recv()
    leave(od, od_out)
    leave(os, os_out)
    for h in range(2):
        value = local(0, h)
        for way in range(2):
            sums[way, h, half - 1].wait_recv()
            value = value + (pr, mr)[way][half - 1, limits[h], :].astype(F32)
        mixed[limits[h], :] = value.astype(BF)
    for copy in outs:
        copy.wait()
    for copy in sent:
        copy.wait_send()


VM = pl.BlockSpec(memory_space=pltpu.VMEM)
ANY = pl.BlockSpec(memory_space=pl.ANY)


def shape(*dims, kind=BF):
    return jax.ShapeDtypeStruct(dims, kind)


def per_device(
    tokens, routes, route_weights, norm_gain, gate_experts, up_experts, down_experts, shared_gate, shared_up, shared_down
):
    fs_count, cols = lax.axis_size("fs"), lax.axis_size("tp")
    chips = fs_count // 2
    experts, span, lanes = gate_experts.shape
    held = experts // fs_count
    toks, quarter = tokens.shape
    top = routes.shape[1]
    dspan = down_experts.shape[1]
    wide = quarter // 2

    def pairs_of(w):
        return w.reshape(fs_count, held, *w.shape[1:])

    def dma(*dims):
        return pltpu.SemaphoreType.DMA(dims)

    slots = chips * 2 * SLOTS
    half = chips // 2
    parts = 4
    rows = toks + META + span // 2 + dspan
    full, dfull = fs_count * span, fs_count * dspan
    ring = [pltpu.VMEM((half, toks, quarter), BF)] * 4
    mixed, gate_ready, up_ready, od, os, sg, su = pl.pallas_call(
        functools.partial(whole_kernel, chips, cols, held, top),
        out_shape=(
            shape(toks, quarter), shape(held, full, lanes), shape(held, full, lanes), shape(held, lanes, quarter * cols),
            shape(lanes, quarter * cols), shape(full, lanes), shape(full, lanes),
        ),
        in_specs=[VM] * 7 + [ANY] * 3,
        out_specs=(VM,) + (ANY,) * 6,
        scratch_shapes=[
            pltpu.VMEM((fs_count, span, lanes), F32), pltpu.VMEM((fs_count, span, lanes), F32),
            pltpu.VMEM((fs_count, dspan, quarter), F32),
            pltpu.VMEM((fs_count, span, 2 * lanes), BF), pltpu.VMEM((fs_count, dspan, quarter), BF),
            pltpu.VMEM((wide, 128), F32), pltpu.VMEM((full, 2 * lanes), BF), pltpu.VMEM((full, 2 * lanes), BF),
            pltpu.VMEM((held, lanes, quarter * cols), BF), pltpu.VMEM((lanes, quarter * cols), BF),
            pltpu.VMEM((full, lanes), BF), pltpu.VMEM((full, lanes), BF), dma(3), dma(8),
            pltpu.VMEM((cols, toks, quarter), BF), pltpu.VMEM((cols, toks, quarter), BF),
            pltpu.VMEM((chips, 2, rows, quarter), BF), pltpu.VMEM((wide, wide), BF),
            pltpu.VMEM((cols, held, slots, quarter), BF), pltpu.VMEM((chips, 2, 4 * SLOTS, wide), BF),
            pltpu.VMEM((dfull, quarter), BF), pltpu.VMEM((dfull, quarter), BF), pltpu.VMEM((dfull, quarter), BF),
            pltpu.VMEM((held, slots, lanes * cols), BF), pltpu.VMEM((toks, lanes * cols), BF),
            pltpu.VMEM((held, slots // parts, quarter), BF), pltpu.VMEM((chips, toks, quarter), F32),
            pltpu.VMEM((chips, toks, quarter), BF), pltpu.VMEM((chips, toks, quarter), BF), *ring,
            dma(chips, 2), dma(chips, 2), dma(chips, 2), dma(chips, 2), dma(chips), dma(chips), dma(chips), dma(chips),
            dma(4), dma(4), dma(2, 2, half), dma(2, 2, half), dma(chips, 2), dma(chips, 2),
            *[dma(chips)] * 6, *[dma(parts + 1)] * 6, dma(chips), dma(chips), dma(2, 2, half), dma(2, 2, half),
            dma(3, cols - 1), dma(3, cols - 1),
        ],
        compiler_params=pltpu.CompilerParams(collective_id=1, has_side_effects=True, vmem_limit_bytes=62 * 2**20),
        cost_estimate=pl.CostEstimate(flops=60_000_000_000, bytes_accessed=16_000_000, transcendentals=0),
    )(
        tokens, routes, route_weights, norm_gain.reshape(span, 1), shared_gate, shared_up, shared_down,
        pairs_of(gate_experts), pairs_of(up_experts), pairs_of(down_experts),
    )
    return mixed, gate_ready, up_ready, od, sg, su, os


def solution(mesh):
    return jax.shard_map(
        per_device,
        mesh=mesh,
        in_specs=(
            P(("grp", "fs"), "tp"), P(("grp", "fs"), None), P(("grp", "fs"), None), P("fs"),
            P(None, "fs", "tp"), P(None, "fs", "tp"), P(None, "fs", "tp"),
            P("fs", "tp"), P("fs", "tp"), P("fs", "tp"),
        ),
        out_specs=(
            P(("grp", "fs"), "tp"), P(("grp", "fs"), None, "tp"), P(("grp", "fs"), None, "tp"),
            P(("grp", "fs"), "tp", None), P("grp", "tp"), P("grp", "tp"), P(("grp", "tp"), None),
        ),
        check_vma=False,
    )
```

time: 302 us -> 220 us (0.73)
  waiting for transfers between devices: 44.6 us -> 0 us
  starting transfers between devices: 30.2 us -> 0 us
  blocking collectives: 7.52 us -> 0 us
  other arithmetic: 6.54 us -> 0 us
  Pallas kernels: 198 us -> 204 us
    all_to_all x2 -> x0, waiting for transfers between devices: 44.6 us -> none  [the longest x1 44.6 us: per_device(): lax.all_to_all(gu_cast, 'fs', 0, 0, tiled=True)]
    all_to_all x2 -> x0, starting transfers between devices: 30.2 us -> none  [the longest x1 24.7 us: per_device(): lax.all_to_all(gu_cast, 'fs', 0, 0, tiled=True)]
    psum x1 -> x0, blocking collectives: 7.52 us -> none  [per_device(): lax.psum(jnp.sum(widened * widened, axis=1, keepdims=True), 'tp')]
    pallas_call x2 -> x1, Pallas kernels: 198 us -> 204 us  [per_device(): pl.pallas_call(functools.partial(whole_kernel, chips, cols, held, top), o...]
    another operation x5 -> x0, other arithmetic: 4.26 us -> none
    unnamed x47 -> x19, local copies, waits for them, and re-layouts: 8.38 us -> 11.4 us
  transfers between devices with their start and end apart: 2 -> 0, of which waited for: 1 -> 0; matrix products, arithmetic and copies ran while one was open for 1% -> 0% of each run, Pallas kernels for 38% -> 0%
where the time goes in v2:
time: 220 us; the launch traced here: 218 us
  Pallas kernels  204 us (93%)
  local copies, waits for them, and re-layouts  12.7 us (6%)
    pallas_call x1, Pallas kernels, per_device(): pl.pallas_call(functools.partial(whole_kernel, chips, cols, held, top), o...  204 us
    unnamed x19, local copies, waits for them, and re-layouts  11.4 us

profile of v2, /device:TPU:38, one launch (start us, length us, event | category | flops | bytes accessed | tf_op | source)
XLA Modules:
  0.0 217.6 jit_solution(6213073225814972509)
XLA Ops:
  0.6 1.4 copy.19.gain
  2.0 1.5 copy.17.routes
  3.5 1.5 copy.18.weights_of
  4.9 204.3 %shard_map.153 = (bf16[224,512]{1,0:T(8,128)(2,1)}, bf16[2,2048,128]{2,1,0:T(8,128)(2,1)}, bf16[2,2048,128]{2,1,0:T(8,128)(2,1)}, bf16[2,128,2048]{2,1,0:T(8,128...) custom-call(bf16[224,512]{1,0:T(8,128)(2,1)} %tok.1, ...), custom_call_target="tpu_custom_call" | custom-call | flops 60000002048 | bytes 16000000 | tf_op jit(solution)/shard_map/pallas_call | solution.py:530
  209.2 0.0 copy-start.1
  209.2 1.7 copy.27
  210.9 0.0 copy-start
  210.9 2.4 %copy.28 = bf16[2,2048,128]{2,1,0:T(8,128)(2,1)} copy(bf16[2,2048,128]{2,1,0:T(8,128)(2,1)} %get-tuple-element.29) | data formatting | bytes 2097152
  213.3 0.0 copy-done.1
  213.3 0.0 copy-start.4
  213.3 1.0 copy.29
  214.3 0.0 copy-done
  214.3 0.0 copy-start.3
  214.3 0.0 copy-start.2
  214.3 1.0 copy.30
  215.2 0.0 copy-done.4
  215.3 0.8 copy.31
  216.0 0.0 copy-done.3
  216.0 0.8 copy.32
  216.8 0.0 copy-done.2
  216.8 0.8 copy.33
Async XLA Ops:
  209.2 4.1 %copy-start.1 = (bf16[2,2048,128]{2,1,0:T(8,128)(2,1)S(1)}, bf16[2,2048,128]{2,1,0:T(8,128)(2,1)}, u32[]{:S(2)}) copy-start(bf16[2,2048,128]{2,1,0:T(8,128)(2,1)} %get-tuple-element.30) | copy-start | bytes 3145732
  210.9 3.3 %copy-start = (bf16[2,128,2048]{2,1,0:T(8,128)(2,1)S(1)}, bf16[2,128,2048]{2,1,0:T(8,128)(2,1)}, u32[]{:S(2)}) copy-start(bf16[2,128,2048]{2,1,0:T(8,128)(2,1)} %get-tuple-element.31) | copy-start | bytes 3145732
  213.3 2.0 copy-start.4
  214.3 1.8 copy-start.3
  214.3 2.6 %copy-start.2 = (bf16[128,2048]{1,0:T(8,128)(2,1)S(1)}, bf16[128,2048]{1,0:T(8,128)(2,1)}, u32[]{:S(2)}) copy-start(bf16[128,2048]{1,0:T(8,128)(2,1)} %get-tuple-element.34) | copy-start | bytes 1572868

commit v3 on v2

--- a/solution.py
+++ b/solution.py
@@ -122,14 +122,16 @@
         return go(remote(here, there, sends.at[delta], recvs.at[delta], grp=pair))
 
     table[...] = jnp.full(table.shape, -1.0, F32)
-    table[0:toks, 0:top] = routes[...].astype(F32)
-    table[0:toks, 8 : 8 + top] = weights_of[...]
-    turned = table[...].T
+    table[0:top, 0:toks] = routes[...].astype(F32)
+    table[8 : 8 + top, 0:toks] = weights_of[...]
+    turned = table[...]
+    diagonal = lax.broadcasted_iota(jnp.int32, (span, span), 0) == lax.broadcasted_iota(jnp.int32, (span, span), 1)
+    column = jnp.sum(jnp.where(diagonal, jnp.broadcast_to(gain[...], (span, span)), 0.0), axis=1, keepdims=True)
     weight = turned[8:16, :]
     high = weight.astype(BF)
     low = (weight - high.astype(F32)).astype(BF)
     short = span // 2
-    scaled = [(v[...] * gain[...]).astype(BF) for v in (sgate_own, sup_own)]
+    scaled = [(v[...] * column).astype(BF) for v in (sgate_own, sup_own)]
     buf[0, c, toks : toks + 8, 0:wide] = turned[0:8, :].astype(BF)
     buf[0, c, toks : toks + 8, wide:] = high
     buf[0, c, toks + 8 : toks + META, 0:wide] = low
@@ -144,8 +146,8 @@
 
     @pl.loop(0, fs_count)
     def _(i):
-        gcast[i, :, 0:lanes] = (gf[i] * gain[...]).astype(BF)
-        gcast[i, :, lanes:] = (uf[i] * gain[...]).astype(BF)
+        gcast[i, :, 0:lanes] = (gf[i] * column).astype(BF)
+        gcast[i, :, lanes:] = (uf[i] * column).astype(BF)
         dcast[i] = df[i].astype(BF)
 
     answered()
@@ -302,20 +304,21 @@
             hand_gates(later)
         if d == half - 1:
             hand_downs()
-        pass_waiting()
-        settle([chips - d, d] if d < half else [half])
+        if d < half:
+            pass_waiting()
+            settle([chips - d, d])
+        else:
+            settle([half])
         for n in ready.get(d, ()):
             swap_ring(n)
     onward[pos[half]] = go(
         remote(block(t, pos[half]), block(t, pos[half]), fs_.at[pos[half]], fr.at[pos[half]], tp=opposite)
     )
+    waiting.remove(pos[half])
+    pass_waiting()
     for n in range(1, half + 1):
         if n not in sum(ready.values(), ()):
             swap_ring(n)
-    to_right[pos[half]].wait_recv()
-    to_left[pos[half]].wait_recv()
-    for p in onward:
-        onward[p].wait_recv()
     down_swaps = []
 
     def land_downs(d):
@@ -327,7 +330,13 @@
                 remote(part(dn, other, dspan), part(dn, other, dspan), ds_.at[0, 0], dr.at[0, 0], fs=other).wait_recv()
             down_swaps.append(swap_chip(dn, dn2, dspan, dys, dyr, delta))
 
-    for d in range(half // 2):
+    for d in range(3):
+        land_downs(d)
+    to_right[pos[half]].wait_recv()
+    to_left[pos[half]].wait_recv()
+    for p in onward:
+        onward[p].wait_recv()
+    for d in range(3, half // 2 + 1):
         land_downs(d)
 
     own_lanes = pl.ds(pl.multiple_of(t * lanes, lanes), lanes)
@@ -344,6 +353,7 @@
 
     for delta in gate_swaps:
         gate_swaps[delta].wait_recv()
+    land_downs(half // 2 + 1)
     outs = []
 
     def leave(src, dst):
@@ -391,13 +401,9 @@
             placed.append(go(remote(source.at[rows_of, :], target.at[:, home], ws.at[kind, k], wr.at[kind, k], tp=a)))
         target[:, home] = source[pl.ds(pl.multiple_of(t * lanes, lanes), lanes), :]
 
-    land_downs(half // 2)
-    land_downs(half // 2 + 1)
+    for d in range(half // 2 + 2, half + 1):
+        land_downs(d)
     pass_act(0)
-    land_downs(half // 2 + 2)
-    pass_act(1)
-    for d in range(half // 2 + 3, half + 1):
-        land_downs(d)
     for copy in down_swaps:
         copy.wait_recv()
     sibs = {}
@@ -455,9 +461,10 @@
 
     done = 1
     for i in range(parts):
-        if i + 2 <= parts:
-            pass_act(i + 2)
         chunk(i)
+        if i == 0:
+            pass_act(1)
+            pass_act(2)
         while done < half and max(pos[half - done], pos[(half + done) % chips]) < (i + 1) * per and done <= 2 * i:
             step(done)
             done += 1
@@ -471,6 +478,8 @@
                 these = pl.ds(n * lanes, lanes)
                 leave(mine.at[:, these], target.at[par])
                 leave(theirs.at[:, these], target.at[1 - par])
+            pass_act(3)
+            pass_act(4)
             leave(sg, sg_out)
             leave(su, su_out)
     onward2[parts].wait_recv()
@@ -503,6 +512,32 @@
     return jax.ShapeDtypeStruct(dims, kind)
 
 
+def finish_kernel(count, *refs):
+    ins, outs, bufs = refs[:count], refs[count : 2 * count], refs[2 * count : 3 * count]
+    in_sem, out_sem = refs[3 * count :]
+    reads = [pltpu.make_async_copy(ins[n], bufs[n], in_sem.at[n]) for n in range(count)]
+    writes = [pltpu.make_async_copy(bufs[n], outs[n], out_sem.at[n]) for n in range(count)]
+    for copy in reads:
+        copy.start()
+    for n in range(count):
+        reads[n].wait()
+        writes[n].start()
+    for copy in writes:
+        copy.wait()
+
+
+def finish(*arrays):
+    count = len(arrays)
+    sems = [pltpu.SemaphoreType.DMA((count,))] * 2
+    return pl.pallas_call(
+        functools.partial(finish_kernel, count),
+        out_shape=tuple(shape(*a.shape, kind=a.dtype) for a in arrays),
+        in_specs=[ANY] * count,
+        out_specs=(ANY,) * count,
+        scratch_shapes=[pltpu.VMEM(a.shape, a.dtype) for a in arrays] + sems,
+    )(*arrays)
+
+
 def per_device(
     tokens, routes, route_weights, norm_gain, gate_experts, up_experts, down_experts, shared_gate, shared_up, shared_down
 ):
@@ -539,7 +574,7 @@
             pltpu.VMEM((fs_count, span, lanes), F32), pltpu.VMEM((fs_count, span, lanes), F32),
             pltpu.VMEM((fs_count, dspan, quarter), F32),
             pltpu.VMEM((fs_count, span, 2 * lanes), BF), pltpu.VMEM((fs_count, dspan, quarter), BF),
-            pltpu.VMEM((wide, 128), F32), pltpu.VMEM((full, 2 * lanes), BF), pltpu.VMEM((full, 2 * lanes), BF),
+            pltpu.VMEM((16, wide), F32), pltpu.VMEM((full, 2 * lanes), BF), pltpu.VMEM((full, 2 * lanes), BF),
             pltpu.VMEM((held, lanes, quarter * cols), BF), pltpu.VMEM((lanes, quarter * cols), BF),
             pltpu.VMEM((full, lanes), BF), pltpu.VMEM((full, lanes), BF), dma(3), dma(8),
             pltpu.VMEM((cols, toks, quarter), BF), pltpu.VMEM((cols, toks, quarter), BF),
@@ -557,10 +592,10 @@
         compiler_params=pltpu.CompilerParams(collective_id=1, has_side_effects=True, vmem_limit_bytes=62 * 2**20),
         cost_estimate=pl.CostEstimate(flops=60_000_000_000, bytes_accessed=16_000_000, transcendentals=0),
     )(
-        tokens, routes, route_weights, norm_gain.reshape(span, 1), shared_gate, shared_up, shared_down,
+        tokens, routes.T, route_weights.T, norm_gain.reshape(1, span), shared_gate, shared_up, shared_down,
         pairs_of(gate_experts), pairs_of(up_experts), pairs_of(down_experts),
     )
-    return mixed, gate_ready, up_ready, od, sg, su, os
+    return finish(mixed, gate_ready, up_ready, od, sg, su, os)
 
 
 def solution(mesh):

time: 220 us -> 217 us (0.986)
  local copies, waits for them, and re-layouts: 12.7 us -> 0 us
  Pallas kernels: 204 us -> 216 us
    unnamed x19 -> x0, local copies, waits for them, and re-layouts: 11.4 us -> none
    pallas_call x1, Pallas kernels: 204 us -> 212 us  [per_device(): pl.pallas_call(functools.partial(whole_kernel, chips, cols, held, top), o...]
    pallas_call x0 -> x1, Pallas kernels: none -> 4.02 us  [finish(): pl.pallas_call(functools.partial(finish_kernel, count), out_shape=tuple((...]
where the time goes in v3:
time: 217 us; the launch traced here: 216 us
  Pallas kernels  216 us (100%)
    pallas_call x1, Pallas kernels, per_device(): pl.pallas_call(functools.partial(whole_kernel, chips, cols, held, top), o...  212 us

profile of v3, /device:TPU:38, one launch (start us, length us, event | category | flops | bytes accessed | tf_op | source)
XLA Modules:
  0.0 216.5 jit_solution(7298147668145978923)
XLA Ops:
  0.6 211.6 %shard_map.153 = (bf16[224,512]{1,0:T(8,128)(2,1)}, bf16[2,2048,128]{2,1,0:T(8,128)(2,1)}, bf16[2,2048,128]{2,1,0:T(8,128)(2,1)}, bf16[2,128,2048]{2,1,0:T(8,128...) custom-call(bf16[224,512]{1,0:T(8,128)(2,1)} %tok.1, s32[6,224]{1,0:T(8,128)} %bitcast.9, ...), custom_call_target="tpu_custom_call" | custom-call | flops 60000002048 | bytes 16000000 | tf_op jit(solution)/shard_map/pallas_call | solution.py:565
  212.3 4.0 %shard_map.154 = (bf16[224,512]{1,0:T(8,128)(2,1)}, bf16[2,2048,128]{2,1,0:T(8,128)(2,1)}, bf16[2,2048,128]{2,1,0:T(8,128)(2,1)}, bf16[2,128,2048]{2,1,0:T(8,128...) custom-call(bf16[224,512]{1,0:T(8,128)(2,1)} %get-tuple-element.14.refs_0_, ...), custom_call_target="tpu_custom_call" | custom-call | tf_op jit(solution)/shard_map/pallas_call | solution.py:532

commit v4 on v3

--- a/solution.py
+++ b/solution.py
@@ -285,7 +285,7 @@
     ready = {half // 2: (1,), half // 2 + 1: (2, 3), half - 2: (4,), half - 1: (5,), half: (6,)} if half == 8 else {}
 
     def hand_downs():
-        for d in range(1, half + 1):
+        for d in range(half, 0, -1):
             for delta in sorted({d, chips - d}):
                 for k in range(2):
                     hand(dcast, dn, dspan, ds_, dr, delta, k)
@@ -322,6 +322,7 @@
     down_swaps = []
 
     def land_downs(d):
+        d = half + 1 - d if d else 0
         for delta in sorted({d, chips - d} if d else {0}):
             if delta:
                 for k in range(2):

time: 217 us -> 217 us (level)
  no operation moved by 1% of the time
where the time goes in v4:
time: 217 us
  Pallas kernels  216 us (100%)
    pallas_call x1, Pallas kernels, per_device(): pl.pallas_call(functools.partial(whole_kernel, chips, cols, held, top), o...  212 us

profile of v4, /device:TPU:38, one launch (start us, length us, event | category | flops | bytes accessed | tf_op | source)
XLA Modules:
  0.0 217.1 jit_solution(11684334445368526755)
XLA Ops:
  0.6 212.3 %shard_map.153 = (bf16[224,512]{1,0:T(8,128)(2,1)}, bf16[2,2048,128]{2,1,0:T(8,128)(2,1)}, bf16[2,2048,128]{2,1,0:T(8,128)(2,1)}, bf16[2,128,2048]{2,1,0:T(8,128...) custom-call(bf16[224,512]{1,0:T(8,128)(2,1)} %tok.1, s32[6,224]{1,0:T(8,128)} %bitcast.9, ...), custom_call_target="tpu_custom_call" | custom-call | flops 60000002048 | bytes 16000000 | tf_op jit(solution)/shard_map/pallas_call | solution.py:566
  212.9 4.0 %shard_map.154 = (bf16[224,512]{1,0:T(8,128)(2,1)}, bf16[2,2048,128]{2,1,0:T(8,128)(2,1)}, bf16[2,2048,128]{2,1,0:T(8,128)(2,1)}, bf16[2,128,2048]{2,1,0:T(8,128...) custom-call(bf16[224,512]{1,0:T(8,128)(2,1)} %get-tuple-element.14.refs_0_, ...), custom_call_target="tpu_custom_call" | custom-call | tf_op jit(solution)/shard_map/pallas_call | solution.py:533
